TPU v7x, 128 devices: a whole 4x4x4 slice. The times are simulated.
128 devices in a mesh: kv: 16 (over z, x), tp: 8 (over y, core).
Axes of the slice: x: 4, y: 4, z: 4, core: 2. Of those that a mesh axis runs over, the one named last changes fastest.
Arguments:
- tokens: bfloat16 [128, 4096], P('tp', 'kv'), may hold values from -16 to 16
- cache_keys: bfloat16 [128, 16384, 2, 128], P('tp', 'kv'), may hold values from -512 to 512
- cache_values: bfloat16 [128, 16384, 2, 128], P('tp', 'kv'), may hold values from -6 to 6
- attn_gain: float32 [4096], P('kv'), may hold values from 0.1 to 1.9
- w_query: bfloat16 [4096, 2048], P('kv'), may hold values from -0.15625 to 0.15625
- w_key: bfloat16 [4096, 256], P('kv'), may hold values from -0.09375 to 0.09375
- w_value: bfloat16 [4096, 256], P('kv'), may hold values from -0.09375 to 0.09375
- lambdas: float32 [16], replicated, may hold values from 0.3 to 0.8
- head_gain: float32 [128], replicated, may hold values from 0.1 to 1.9
- w_out: bfloat16 [2048, 4096], P(None, 'kv'), may hold values from -0.125 to 0.125
- mlp_gain: float32 [4096], P('kv'), may hold values from 0.1 to 1.9
- w_up: bfloat16 [4096, 16384], P('kv', 'tp'), may hold values from -0.09375 to 0.09375
- w_down: bfloat16 [16384, 4096], P('tp', 'kv'), may hold values from -0.046875 to 0.046875
Outputs:
- mixed: bfloat16 [128, 4096], P('tp', 'kv')
- new_keys: bfloat16 [128, 2, 128], P('tp')
- new_values: bfloat16 [128, 2, 128], P('tp')
All inputs are finite; a program needn't handle non-finite values.
Results may differ from a plain program's by a relative error of at most 0.014.
Values may be sent and summed in bfloat16 or wider, within the bound.
A program may use at most 128 MiB of HBM per device.

v0:
```python
import functools

import jax
import jax.numpy as jnp
from jax import lax
from jax.experimental import pallas as pl
from jax.experimental.pallas import tpu as pltpu
from jax.sharding import PartitionSpec as P

norm_eps = 1e-06
f32 = jnp.float32
bf16 = jnp.bfloat16
VM = pl.BlockSpec(memory_space=pltpu.VMEM)
ANY = pl.BlockSpec(memory_space=pl.ANY)
DMA = pltpu.SemaphoreType.DMA


def greet(axis, n, me):
    barrier = pltpu.get_barrier_semaphore()
    for k in range(1, n):
        pl.semaphore_signal(
            barrier, inc=1, device_id={axis: lax.rem(me + k, n)}, device_id_type=pl.DeviceIdType.MESH
        )
    pl.semaphore_wait(barrier, n - 1)


def remote(src, dst, send, recv, axis, peer):
    return pltpu.make_async_remote_copy(
        src_ref=src,
        dst_ref=dst,
        send_sem=send,
        recv_sem=recv,
        device_id={axis: peer},
        device_id_type=pl.DeviceIdType.MESH,
    )


def send_all(axis, n, me, src_of, dst, send, recv):
    for k in range(1, n):
        peer = lax.rem(me + k, n)
        remote(src_of(peer), dst, send.at[peer], recv.at[me], axis, peer).start()


def wait_all(axis, n, me, src_of, slot_of, send, recv):
    for k in range(1, n):
        peer = lax.rem(me + n - k, n)
        remote(src_of(peer), slot_of(peer), send.at[peer], recv.at[peer], axis, peer).wait_recv()


def drain(axis, n, me, src_of, dst, send, recv):
    for k in range(1, n):
        peer = lax.rem(me + k, n)
        remote(src_of(peer), dst, send.at[peer], recv.at[me], axis, peer).wait_send()


def call(body, args, in_specs, out_shape, scratch, cid, out_spec=VM, flops=0, nbytes=0):
    return pl.pallas_call(
        body,
        out_shape=out_shape,
        in_specs=in_specs,
        out_specs=out_spec,
        scratch_shapes=scratch,
        cost_estimate=pl.CostEstimate(flops=flops, bytes_accessed=nbytes, transcendentals=0),
        compiler_params=pltpu.CompilerParams(
            collective_id=cid, has_side_effects=True, vmem_limit_bytes=48 * 1024 * 1024
        ),
    )(*args)


def proj_kernel(n, full_width, part, out, got, mine, s1, r1, s2, r2):
    me = lax.axis_index("kv")
    width = mine.shape[1]
    greet("kv", n, me)
    src = lambda peer: part.at[peer]
    slot = lambda peer: got.at[peer]
    send_all("kv", n, me, src, got.at[me], s1, r1)
    got[me] = part[me]
    wait_all("kv", n, me, src, slot, s1, r1)
    total = got[0]
    for k in range(1, n):
        total = total + got[k]
    inv = lax.rsqrt(total[:, width : width + 1] / full_width + norm_eps)
    mine[...] = (total[:, :width] * inv).astype(bf16)
    own = lambda peer: mine
    send_all("kv", n, me, own, out.at[me], s2, r2)
    out[me] = mine[...]
    wait_all("kv", n, me, own, lambda peer: out.at[peer], s2, r2)
    drain("kv", n, me, src, got.at[me], s1, r1)
    drain("kv", n, me, own, out.at[me], s2, r2)


def attn_kernel(
    n,
    rows,
    kv_heads,
    group,
    ctx_total,
    q,
    keys,
    values,
    lam,
    gain,
    out,
    kbuf,
    vbuf,
    acc,
    stat,
    gacc,
    gstat,
    mine,
    ksem,
    vsem,
    sa,
    ra,
    ss,
    rs,
    s2,
    r2,
):
    me = lax.axis_index("kv")
    lines = q.shape[1]
    span = keys.shape[1]

    def dest(j):
        return lax.rem(me + 1 + j, n)

    def fetch(j, slot):
        at = pl.ds(dest(j) * rows, rows)
        return (
            pltpu.make_async_copy(keys.at[at], kbuf.at[slot], ksem.at[slot]),
            pltpu.make_async_copy(values.at[at], vbuf.at[slot], vsem.at[slot]),
        )

    for c in fetch(0, 0):
        c.start()
    greet("kv", n, me)
    head_of = lax.broadcasted_iota(jnp.int32, (lines, span), 0) // (2 * group)
    col_head = lax.rem(lax.broadcasted_iota(jnp.int32, (lines, span), 1), kv_heads)
    mask = jnp.where(head_of == col_head, 0.0, -jnp.inf).astype(f32)
    lane = lax.broadcasted_iota(jnp.int32, (lines, 128), 1)

    def step(j, carry):
        slot = lax.rem(j, 2)
        d = dest(j)

        @pl.when(j + 1 < n)
        def _():
            for c in fetch(j + 1, 1 - slot):
                c.start()

        for c in fetch(j, slot):
            c.wait()
        for i in range(rows):
            s = lax.dot_general(
                q[d * rows + i], kbuf[slot, i], (((1,), (1,)), ((), ())), preferred_element_type=f32
            )
            s = s + mask
            top = jnp.max(s, axis=1, keepdims=True)
            e = jnp.exp(s - top)
            total = jnp.sum(e, axis=1, keepdims=True)
            o = jnp.dot(e.astype(bf16), vbuf[slot, i], preferred_element_type=f32)
            acc[d, i] = o.astype(bf16)
            both = jnp.where(lane == 0, top, total)
            stat[d, i] = jnp.transpose(both)[:8]

        @pl.when(j + 1 < n)
        def _():
            remote(acc.at[d], gacc.at[me], sa.at[d], ra.at[me], "kv", d).start()
            remote(stat.at[d], gstat.at[me], ss.at[d], rs.at[me], "kv", d).start()

        return carry

    lax.fori_loop(0, n, step, 0)
    gacc[me] = acc[me]
    gstat[me] = stat[me]
    wait_all("kv", n, me, lambda p: acc.at[p], lambda p: gacc.at[p], sa, ra)
    wait_all("kv", n, me, lambda p: stat.at[p], lambda p: gstat.at[p], ss, rs)
    for i in range(rows):
        cols = [jnp.transpose(gstat[k, i]) for k in range(n)]
        peak = cols[0][:, 0:1]
        for k in range(1, n):
            peak = jnp.maximum(peak, cols[k][:, 0:1])
        total = 0.0
        merged = 0.0
        for k in range(n):
            fac = jnp.exp(cols[k][:, 0:1] - peak)
            total = total + fac * cols[k][:, 1:2]
            merged = merged + fac * gacc[k, i].astype(f32)
        ratio = merged / total
        for g in range(kv_heads):
            base = g * 2 * group
            head = (
                ratio[base : base + group]
                - lam[g * group : (g + 1) * group, 0:1] * ratio[base + group : base + 2 * group]
            )
            mean_sq = jnp.mean(head * head, axis=1, keepdims=True)
            normed = head * lax.rsqrt(mean_sq + 1.0 / ctx_total) * gain[0:1, :]
            mine[i, g * group : (g + 1) * group, :] = normed.astype(bf16)
    own = lambda peer: mine
    send_all("kv", n, me, own, out.at[me], s2, r2)
    out[me] = mine[...]
    wait_all("kv", n, me, own, lambda peer: out.at[peer], s2, r2)
    for k in range(1, n):
        p = lax.rem(me + k, n)
        remote(acc.at[p], gacc.at[me], sa.at[p], ra.at[me], "kv", p).wait_send()
        remote(stat.at[p], gstat.at[me], ss.at[p], rs.at[me], "kv", p).wait_send()
    drain("kv", n, me, own, out.at[me], s2, r2)


def act_kernel(n, full_width, part, sq, out, got, gsq, mine, s0, r0, s1, r1, s2, r2):
    me = lax.axis_index("kv")
    cw = mine.shape[1]
    greet("kv", n, me)

    def cols(k):
        return pl.ds(pl.multiple_of(k * cw, cw), cw)

    src = lambda peer: part.at[:, cols(peer)]
    one = lambda peer: sq
    send_all("kv", n, me, one, gsq.at[me], s0, r0)
    send_all("kv", n, me, src, got.at[me], s1, r1)
    gsq[me] = sq[...]
    got[me] = part[:, cols(me)]
    wait_all("kv", n, me, one, lambda p: gsq.at[p], s0, r0)
    sums = gsq[0]
    for k in range(1, n):
        sums = sums + gsq[k]
    inv = lax.rsqrt(jnp.transpose(sums)[:, 0:1] / full_width + norm_eps)
    wait_all("kv", n, me, src, lambda p: got.at[p], s1, r1)
    total = got[0].astype(f32)
    for k in range(1, n):
        total = total + got[k].astype(f32)
    pre = jnp.maximum(total * inv, 0.0)
    mine[...] = (pre * pre).astype(bf16)
    own = lambda peer: mine
    send_all("kv", n, me, own, out.at[:, cols(me)], s2, r2)
    out[:, cols(me)] = mine[...]
    wait_all("kv", n, me, own, lambda p: out.at[:, cols(p)], s2, r2)
    drain("kv", n, me, one, gsq.at[me], s0, r0)
    drain("kv", n, me, src, got.at[me], s1, r1)
    drain("kv", n, me, own, out.at[:, cols(me)], s2, r2)


def down_kernel(n, part, res, out, got, s1, r1):
    me = lax.axis_index("tp")
    rows = res.shape[0]
    greet("tp", n, me)
    src = lambda peer: part.at[pl.ds(pl.multiple_of(peer * rows, rows), rows)]
    send_all("tp", n, me, src, got.at[me], s1, r1)
    got[me] = part[pl.ds(pl.multiple_of(me * rows, rows), rows), :]
    wait_all("tp", n, me, src, lambda p: got.at[p], s1, r1)
    total = got[0].astype(f32)
    for k in range(1, n):
        total = total + got[k].astype(f32)
    out[...] = (res[...].astype(f32) + total).astype(bf16)
    drain("tp", n, me, src, got.at[me], s1, r1)


def shards(
    tokens,
    cache_keys,
    cache_values,
    attn_gain,
    w_query,
    w_key,
    w_value,
    lambdas,
    head_gain,
    w_out,
    mlp_gain,
    w_up,
    w_down,
):
    B, tok_width = tokens.shape
    n = lax.axis_size("kv")
    n_tp = lax.axis_size("tp")
    full_width = tok_width * n
    kv_heads = cache_keys.shape[2]
    comp = cache_keys.shape[3] // 2
    vd = cache_values.shape[3]
    ctx = cache_keys.shape[1]
    heads = lambdas.shape[0]
    group = heads // kv_heads
    ctx_total = ctx * n
    rows = B // n
    qw, kw, vw = w_query.shape[1], w_key.shape[1], w_value.shape[1]
    width = qw + kw + vw

    tok_f = tokens.astype(f32)
    scaled = (tok_f * attn_gain[None, :]).astype(bf16)
    squares = jnp.sum(tok_f * tok_f, axis=1, keepdims=True)
    part = jnp.concatenate(
        [jnp.dot(scaled, w, preferred_element_type=f32) for w in (w_query, w_key, w_value)]
        + [jnp.broadcast_to(squares, (B, 128))],
        axis=1,
    ).reshape(n, rows, width + 128)
    sems = [DMA((n,))] * 4
    proj = call(
        functools.partial(proj_kernel, n, full_width),
        (part,),
        [VM],
        jax.ShapeDtypeStruct((n, rows, width), bf16),
        [pltpu.VMEM((n, rows, width + 128), f32), pltpu.VMEM((rows, width), bf16)] + sems,
        0,
    ).reshape(B, width)
    query = proj[:, :qw].reshape(B, kv_heads, group, 2, comp)
    new_keys = proj[:, qw : qw + kw].reshape(B, kv_heads, 2 * comp)
    new_values = proj[:, qw + kw :].reshape(B, kv_heads, vd)
    scale = comp ** (-0.5)
    qs = (query.astype(f32) * scale).astype(bf16)
    zero = jnp.zeros_like(qs[..., 0, :])
    q_lines = jnp.stack(
        [
            jnp.concatenate([qs[..., 0, :], zero], axis=-1),
            jnp.concatenate([zero, qs[..., 1, :]], axis=-1),
        ],
        axis=2,
    ).reshape(B, 2 * heads, 2 * comp)
    lines = 2 * heads
    span = ctx * kv_heads
    lam = jnp.broadcast_to(lambdas[:, None], (heads, 128))
    gain = jnp.broadcast_to(head_gain[None, :], (8, vd))
    normed = call(
        functools.partial(attn_kernel, n, rows, kv_heads, group, ctx_total),
        (
            q_lines,
            cache_keys.reshape(B, span, 2 * comp),
            cache_values.reshape(B, span, vd),
            lam,
            gain,
        ),
        [VM, ANY, ANY, VM, VM],
        jax.ShapeDtypeStruct((n, rows, heads, vd), bf16),
        [
            pltpu.VMEM((2, rows, span, 2 * comp), bf16),
            pltpu.VMEM((2, rows, span, vd), bf16),
            pltpu.VMEM((n, rows, lines, vd), bf16),
            pltpu.VMEM((n, rows, 8, lines), f32),
            pltpu.VMEM((n, rows, lines, vd), bf16),
            pltpu.VMEM((n, rows, 8, lines), f32),
            pltpu.VMEM((rows, heads, vd), bf16),
            DMA((2,)),
            DMA((2,)),
        ]
        + [DMA((n,))] * 6,
        1,
        flops=8 * B * lines * span * vd,
        nbytes=4 * B * span * vd,
    ).reshape(B, heads * vd)
    attn_out = jnp.dot(normed, w_out, preferred_element_type=f32)
    residual = (tok_f + attn_out).astype(bf16)
    everyone = lax.all_gather(residual, "tp", axis=0, tiled=True)
    every_f = everyone.astype(f32)
    gained = (every_f * mlp_gain[None, :]).astype(bf16)
    row_sq = jnp.sum(every_f * every_f, axis=1)
    up_part = jnp.dot(gained, w_up, preferred_element_type=f32).astype(bf16)
    all_rows, hidden = up_part.shape
    cw = hidden // n
    sq = jnp.broadcast_to(row_sq[None, :], (8, all_rows))
    act_rows = call(
        functools.partial(act_kernel, n, full_width),
        (up_part, sq),
        [VM, VM],
        jax.ShapeDtypeStruct((all_rows, hidden), bf16),
        [
            pltpu.VMEM((n, all_rows, cw), bf16),
            pltpu.VMEM((n, 8, all_rows), f32),
            pltpu.VMEM((all_rows, cw), bf16),
        ]
        + [DMA((n,))] * 6,
        2,
    )
    down = jnp.dot(act_rows, w_down, preferred_element_type=f32).astype(bf16)
    mixed = call(
        functools.partial(down_kernel, n_tp),
        (down, residual),
        [VM, VM],
        jax.ShapeDtypeStruct(residual.shape, bf16),
        [pltpu.VMEM((n_tp,) + residual.shape, bf16), DMA((n_tp,)), DMA((n_tp,))],
        3,
    )
    return mixed, new_keys, new_values


def solution(mesh):
    in_specs = (
        P("tp", "kv"),
        P("tp", "kv", None, None),
        P("tp", "kv", None, None),
        P("kv"),
        P("kv", None),
        P("kv", None),
        P("kv", None),
        P(),
        P(),
        P(None, "kv"),
        P("kv"),
        P("kv", "tp"),
        P("tp", "kv"),
    )
    out_specs = (P("tp", "kv"), P("tp", None, None), P("tp", None, None))
    return jax.shard_map(shards, mesh=mesh, in_specs=in_specs, out_specs=out_specs, check_vma=False)
```

profile of v0, /device:TPU:1, one launch (start us, length us, event | category | flops | bytes accessed | tf_op | source)
XLA Modules:
  0.0 96.3 jit_solution(13484259546586129526)
XLA Ops:
  0.6 0.0 copy-start
  0.6 0.9 fusion.8
  1.5 0.7 broadcast_in_dim.10.gain
  2.2 0.1 broadcast_in_dim.8
  2.3 0.7 broadcast_in_dim.9.lam
  3.0 1.1 %fusion.11 = f32[16,256]{1,0:T(8,128)S(1)} fusion(bf16[256,256]{1,0:T(8,128)(2,1)} %param.18, bf16[16,256]{1,0:T(8,128)(2,1)} %param.13, f32[256]{0:T(256)} %param.16), kind=kOutput, calls=%fused_computation.24 | convolution fusion | flops 2109440 | bytes 156672 | tf_op jit(solution)/shard_map/dot_general | solution.py:293
  4.1 1.1 %fusion.9 = f32[16,256]{1,0:T(8,128)S(1)} fusion(bf16[256,256]{1,0:T(8,128)(2,1)} %param.19, bf16[16,256]{1,0:T(8,128)(2,1)} %param.13, f32[256]{0:T(256)} %param.16), kind=kOutput, calls=%fused_computation.23 | convolution fusion | flops 2109440 | bytes 156672 | tf_op jit(solution)/shard_map/dot_general | solution.py:293
  5.2 1.5 %fusion.13 = f32[16,2048]{1,0:T(8,128)S(1)} fusion(bf16[256,2048]{1,0:T(8,128)(2,1)} %param.17, bf16[16,256]{1,0:T(8,128)(2,1)} %param.13, f32[256]{0:T(256)} %param.16), kind=kOutput, calls=%fused_computation.25 | convolution fusion | flops 16789504 | bytes 1188864 | tf_op jit(solution)/shard_map/dot_general | solution.py:293
  6.7 0.1 reshape.41.part
  6.8 16.6 %shard_map.148 = bf16[16,1,2560]{2,1,0:T(2,128)(2,1)S(1)} custom-call(f32[16,1,2688]{2,1,0:T(1,128)S(1)} %reshape.41.part), custom_call_target="tpu_custom_call" | custom-call | tf_op jit(solution)/shard_map/pallas_call | solution.py:57
  23.5 0.6 reshape.48
  24.1 0.6 reshape.47
  24.7 0.2 convert_element_type.35
  24.9 0.2 fusion.15
  25.1 0.1 pad_bitcast_fusion
  25.3 24.1 %shard_map.149 = bf16[16,1,16,128]{3,2,1,0:T(8,128)(2,1)S(1)} custom-call(bf16[16,32,128]{2,1,0:T(8,128)(2,1)S(1)} %bitcast.26, bf16[16,2048,128]{2,1,0:T(8,128)(2,1)} %bitcast.28, bf16[16,2048,128]{2,1,0:T(8,128)(2,1)} %bitcast.29, f32[16,128]{1,0:T(8,128)S(1)} %broadcast_in_dim.9.lam, f32[8,128]{1,0:T(8,128)S(1)} %broadcast_in_dim.10.gain), custom_call_target="tpu_custom_call" | custom-call | flops 1073741824 | bytes 16777216 | tf_op jit(solution)/shard_map/pallas_call | solution.py:57
  49.4 0.2 fusion.res
  49.7 17.8 %all_gather.3 = bf16[128,256]{1,0:T(8,128)(2,1)S(1)} all-gather(bf16[16,256]{1,0:T(8,128)(2,1)S(1)} %fusion.res), channel_id=1, replica_groups=mesh['kv'=16,'tp'=8] {'tp'}, dimensions={0}, use_global_device_ids=true | all-gather | bytes 73728 | tf_op jit(solution)/shard_map/all_gather | solution.py:352
  67.5 0.1 fusion.2
  67.6 0.3 convolution_convert_fusion.part
  68.0 19.6 %shard_map.150 = bf16[128,2048]{1,0:T(8,128)(2,1)S(1)} custom-call(bf16[128,2048]{1,0:T(8,128)(2,1)S(1)} %convolution_convert_fusion.part, f32[8,128]{1,0:T(8,128)S(1)} %broadcast_in_dim.11.sq), custom_call_target="tpu_custom_call" | custom-call | tf_op jit(solution)/shard_map/pallas_call | solution.py:57
  87.6 0.3 convolution_convert_fusion.1.part
  87.9 7.8 %shard_map.151 = bf16[16,256]{1,0:T(8,128)(2,1)S(1)} custom-call(bf16[128,256]{1,0:T(8,128)(2,1)S(1)} %convolution_convert_fusion.1.part, bf16[16,256]{1,0:T(8,128)(2,1)S(1)} %fusion.res), custom_call_target="tpu_custom_call" | custom-call | tf_op jit(solution)/shard_map/pallas_call | solution.py:57
  95.7 0.6 copy.33
  (17 shorter events, 0.1 us)
Async XLA Ops:
  0.6 67.0 %copy-start = (bf16[256,2048]{1,0:T(8,128)(2,1)S(1)}, bf16[256,2048]{1,0:T(8,128)(2,1)}, u32[]{:S(2)}) copy-start(bf16[256,2048]{1,0:T(8,128)(2,1)} %param.24) | copy-start | bytes 3145732
  25.2 24.2 %copy-start.1 = (bf16[2048,256]{1,0:T(8,128)(2,1)S(1)}, bf16[2048,256]{1,0:T(8,128)(2,1)}, u32[]{:S(2)}) copy-start(bf16[2048,256]{1,0:T(8,128)(2,1)} %param.22) | copy-start | bytes 3145732
  25.2 24.2 %copy-start.3 = (bf16[16,256]{1,0:T(8,128)(2,1)S(1)}, bf16[16,256]{1,0:T(8,128)(2,1)}, u32[]{:S(2)}) copy-start(bf16[16,256]{1,0:T(8,128)(2,1)} %param.13) | copy-start | bytes 24580
  25.3 42.4 %copy-start.4 = (f32[256]{0:T(256)S(1)}, f32[256]{0:T(256)}, u32[]{:S(2)}) copy-start(f32[256]{0:T(256)} %param.23) | copy-start | bytes 3076
  25.3 62.3 %copy-start.2 = (bf16[2048,256]{1,0:T(8,128)(2,1)S(1)}, bf16[2048,256]{1,0:T(8,128)(2,1)}, u32[]{:S(2)}) copy-start(bf16[2048,256]{1,0:T(8,128)(2,1)} %param.25) | copy-start | bytes 3145732
where the time goes:
time: 96.8 us; the launch traced here: 96.3 us
  Pallas kernels  68.1 us (70%)
  blocking collectives  17.8 us (18%)
  matrix products  4.56 us (5%)
  local copies, waits for them, and re-layouts  3.93 us (4%)
  other arithmetic  1.05 us (1%)
    pallas_call x4, Pallas kernels, call(): pl.pallas_call(body, out_shape=out_shape, in_specs=in_specs, out_specs=ou...  68.1 us
    all_gather x1, blocking collectives, shards(): everyone = lax.all_gather(residual, 'tp', axis=0, tiled=True)  17.8 us
    dot_general x3, matrix products, shards(): jnp.dot(scaled, w, preferred_element_type=f32)  3.68 us

commit v1 on v0

v1 whole, which is shorter than its diff:
```python
import functools

import jax
import jax.numpy as jnp
from jax import lax
from jax.experimental import pallas as pl
from jax.experimental.pallas import tpu as pltpu
from jax.sharding import PartitionSpec as P

norm_eps = 1e-06
f32 = jnp.float32
bf16 = jnp.bfloat16
VM = pl.BlockSpec(memory_space=pltpu.VMEM)
ANY = pl.BlockSpec(memory_space=pl.ANY)
DMA = pltpu.SemaphoreType.DMA
NT = (((1,), (1,)), ((), ()))
CHUNKS = 2
UNROLL = 2


def remote(src, dst, send, recv, axis, peer):
    return pltpu.make_async_remote_copy(
        src_ref=src,
        dst_ref=dst,
        send_sem=send,
        recv_sem=recv,
        device_id={axis: peer},
        device_id_type=pl.DeviceIdType.MESH,
    )


class Exchange:
    def __init__(self, axis, n, me, src_of, dst_of, send, recv):
        self.axis, self.n, self.me = axis, n, me
        self.src_of, self.dst_of, self.send, self.recv = src_of, dst_of, send, recv

    def copy(self, peer):
        me = self.me
        return remote(
            self.src_of(peer), self.dst_of(me), self.send.at[peer], self.recv.at[me], self.axis, peer
        )

    def start(self, k):
        self.copy(lax.rem(self.me + k, self.n)).start()

    def start_all(self):
        for k in range(1, self.n):
            self.start(k)

    def wait_from(self, peer):
        remote(
            self.src_of(peer), self.dst_of(peer), self.send.at[peer], self.recv.at[peer], self.axis, peer
        ).wait_recv()

    def wait_all(self):
        for k in range(1, self.n):
            self.wait_from(lax.rem(self.me + self.n - k, self.n))

    def drain(self):
        for k in range(1, self.n):
            self.copy(lax.rem(self.me + k, self.n)).wait_send()


def rows_of(start, size):
    return pl.ds(pl.multiple_of(start, size), size)


def layer_kernel(
    n,
    n_tp,
    kv_heads,
    full_width,
    ctx_total,
    scale,
    tokens,
    keys,
    values,
    attn_gain,
    w_query,
    w_key,
    w_value,
    lambdas,
    head_gain,
    w_out,
    mlp_gain,
    w_up,
    w_down,
    mixed,
    kv_out,
    tok_v,
    ag_v,
    wq_v,
    wk_v,
    wv_v,
    lam_v,
    hg_v,
    mg_v,
    kbuf,
    vbuf,
    wo_v,
    wu_v,
    wd_v,
    lsem,
    ksem,
    vsem,
    part_q,
    part_s,
    part_kv,
    got_q,
    got_s,
    got_kv,
    mine_q,
    mine_kv,
    all_q,
    acc,
    stat,
    gacc,
    gstat,
    mine_n,
    all_n,
    norm_f,
    res_v,
    all_res,
    sq_v,
    got_sq,
    up_v,
    got_up,
    mine_act,
    all_act,
    down_v,
    got_down,
    sems16,
    sems8,
    sems_up,
):
    me = lax.axis_index("kv")
    my_tp = lax.axis_index("tp")
    B = tokens.shape[0]
    heads = got_q.shape[1]
    half = heads // kv_heads
    lines = 2 * heads
    span = keys.shape[1]
    cols = tok_v.shape[1]
    all_rows = B * n_tp
    R = all_rows // CHUNKS
    groups = span // 128

    def ex(axis, i, src_of, dst_of):
        if axis == "kv":
            return Exchange("kv", n, me, src_of, dst_of, sems16.at[2 * i], sems16.at[2 * i + 1])
        return Exchange("tp", n_tp, my_tp, src_of, dst_of, sems8.at[2 * i], sems8.at[2 * i + 1])

    first = [(tokens, tok_v), (attn_gain, ag_v), (w_query, wq_v), (w_key, wk_v), (w_value, wv_v)]
    later = [
        (lambdas, lam_v),
        (head_gain, hg_v),
        (w_out, wo_v),
        (mlp_gain, mg_v),
        (w_up, wu_v),
        (w_down, wd_v),
    ]
    first = [pltpu.make_async_copy(a, b, lsem.at[i]) for i, (a, b) in enumerate(first)]
    later = [pltpu.make_async_copy(a, b, lsem.at[len(first) + i]) for i, (a, b) in enumerate(later)]
    for c in first:
        c.start()
    barrier = pltpu.get_barrier_semaphore()
    for axis, size, at in (("kv", n, me), ("tp", n_tp, my_tp)):
        for k in range(1, size):
            pl.semaphore_signal(
                barrier,
                inc=1,
                device_id={axis: lax.rem(at + k, size)},
                device_id_type=pl.DeviceIdType.MESH,
            )
    for c in first:
        c.wait()

    def fetch(b):
        return (
            pltpu.make_async_copy(keys.at[b], kbuf.at[b], ksem.at[b]),
            pltpu.make_async_copy(values.at[b], vbuf.at[b], vsem.at[b]),
        )

    def fetch_step(j, carry):
        for c in fetch(lax.rem(me + 1 + j, n)):
            c.start()
        return carry

    lax.fori_loop(0, B, fetch_step, 0)
    for c in later:
        c.start()

    tok_f = tok_v[...].astype(f32)
    scaled = (tok_f * ag_v[...]).astype(bf16)
    squares = jnp.broadcast_to(jnp.sum(tok_f * tok_f, axis=1, keepdims=True), (B, 128))
    for r in range(B):
        part_s[r] = squares[r : r + 1]
    product = jnp.dot(scaled, wq_v[...], preferred_element_type=f32)
    for h in range(heads):
        part_q[pl.ds(h, B, stride=heads), :] = product[:, h * 128 : (h + 1) * 128]
    pieces = 0
    for w in (wk_v, wv_v):
        product = jnp.dot(scaled, w[...], preferred_element_type=f32)
        for h in range(product.shape[1] // 128):
            part_kv[pl.ds(pieces, B, stride=8), :] = product[:, h * 128 : (h + 1) * 128]
            pieces += 1
    for h in range(pieces, 8):
        part_kv[pl.ds(h, B, stride=8), :] = jnp.zeros((B, 128), f32)

    x_q = ex("kv", 0, lambda p: part_q.at[rows_of(p * heads, heads)], lambda p: got_q.at[p])
    x_s = ex("kv", 1, lambda p: part_s.at[p], lambda p: got_s.at[p])
    x_kv = ex("kv", 2, lambda p: part_kv.at[rows_of(p * 8, 8)], lambda p: got_kv.at[p])
    pl.semaphore_wait(barrier, n - 1 + n_tp - 1)
    for k in range(1, n):
        x_s.start(k)
        x_q.start(k)
    x_kv.start_all()
    got_q[me] = part_q[rows_of(me * heads, heads), :]
    got_s[me] = part_s[me]
    got_kv[me] = part_kv[rows_of(me * 8, 8), :]
    x_s.wait_all()
    total = got_s[0]
    for k in range(1, n):
        total = total + got_s[k]
    inv_one = lax.rsqrt(total / full_width + norm_eps)
    x_q.wait_all()
    total = got_q[0]
    for k in range(1, n):
        total = total + got_q[k]
    query = (total * inv_one).astype(bf16).astype(f32) * scale
    mine_q[...] = query.astype(bf16)
    x_q2 = ex("kv", 3, lambda p: mine_q, lambda p: all_q.at[p])
    x_q2.start_all()
    all_q[me] = mine_q[...]
    x_kv.wait_all()
    total = got_kv[0]
    for k in range(1, n):
        total = total + got_kv[k]
    mine_kv[...] = (total * inv_one).astype(bf16)
    x_kv2 = ex("kv", 4, lambda p: mine_kv, lambda p: kv_out.at[p])
    x_kv2.start_all()
    kv_out[me] = mine_kv[...]

    lane = lax.broadcasted_iota(jnp.int32, (heads, 128), 1)
    even = lax.rem(lane, 2) == 0
    low = lane < 64
    diag = lax.broadcasted_iota(jnp.int32, (lines, 128), 1) == lax.broadcasted_iota(
        jnp.int32, (lines, 128), 0
    )

    x_acc = ex("kv", 5, lambda p: acc.at[p], lambda p: gacc.at[p])
    x_stat = ex("kv", 6, lambda p: stat.at[p], lambda p: gstat.at[p])

    def dest(j):
        return lax.rem(me + 1 + j, n)

    def one_row(b):
        q = all_q[b].astype(f32)
        lo = jnp.where(low, q, 0.0)
        hi = jnp.where(low, 0.0, q)
        q_lines = jnp.concatenate([lo[:half], hi[:half], lo[half:], hi[half:]], axis=0).astype(bf16)
        s = lax.dot_general(q_lines, kbuf[b], NT, preferred_element_type=f32)
        m = [
            jnp.where(even, s[:heads, c * 128 : (c + 1) * 128], s[heads:, c * 128 : (c + 1) * 128])
            for c in range(groups)
        ]
        top = m[0]
        for c in range(1, groups):
            top = jnp.maximum(top, m[c])
        top0 = jnp.max(jnp.where(even, top, -jnp.inf), axis=1, keepdims=True)
        top1 = jnp.max(jnp.where(even, -jnp.inf, top), axis=1, keepdims=True)
        top = jnp.where(even, top0, top1)
        m = [jnp.exp(x - top) for x in m]
        total = m[0]
        for c in range(1, groups):
            total = total + m[c]
        tot0 = jnp.sum(jnp.where(even, total, 0.0), axis=1, keepdims=True)
        tot1 = jnp.sum(jnp.where(even, 0.0, total), axis=1, keepdims=True)
        e = jnp.concatenate(
            [
                jnp.concatenate([jnp.where(even, x, 0.0).astype(bf16) for x in m], axis=1),
                jnp.concatenate([jnp.where(even, 0.0, x).astype(bf16) for x in m], axis=1),
            ],
            axis=0,
        )
        o = jnp.dot(e, vbuf[b], preferred_element_type=f32)
        tops = jnp.concatenate([top0, top1], axis=0)
        tots = jnp.concatenate([tot0, tot1], axis=0)
        row0 = jnp.sum(jnp.where(diag, tops, 0.0), axis=0, keepdims=True)
        row1 = jnp.sum(jnp.where(diag, tots, 0.0), axis=0, keepdims=True)
        return o.astype(bf16), jnp.concatenate([row0, row1], axis=0)

    def step(i, carry):
        bs = [dest(i * UNROLL + u) for u in range(UNROLL)]
        for u, b in enumerate(bs):
            if u == UNROLL - 1:

                @pl.when(b != me)
                def _(b=b):
                    x_q2.wait_from(b)

            else:
                x_q2.wait_from(b)
            for c in fetch(b):
                c.wait()
        results = [one_row(b) for b in bs]
        for u, (b, (o, st)) in enumerate(zip(bs, results)):
            acc[b] = o
            stat[b] = st
        for u, b in enumerate(bs):
            if u == UNROLL - 1:

                @pl.when(b != me)
                def _(b=b):
                    x_acc.copy(b).start()
                    x_stat.copy(b).start()

            else:
                x_acc.copy(b).start()
                x_stat.copy(b).start()
        return carry

    lax.fori_loop(0, B // UNROLL, step, 0)
    gacc[me] = acc[me]
    gstat[me] = stat[me]
    for c in later:
        c.wait()
    lam = jnp.broadcast_to(lam_v[...], (heads, heads))
    lam = jnp.sum(
        jnp.where(
            lax.broadcasted_iota(jnp.int32, (heads, heads), 0)
            == lax.broadcasted_iota(jnp.int32, (heads, heads), 1),
            lam,
            0.0,
        ),
        axis=1,
        keepdims=True,
    )
    x_stat.wait_all()
    tops = [gstat[k][0:1] for k in range(n)]
    peak = tops[0]
    for t in tops[1:]:
        peak = jnp.maximum(peak, t)
    facs = [jnp.exp(t - peak) for t in tops]
    total = facs[0] * gstat[0][1:2]
    for k in range(1, n):
        total = total + facs[k] * gstat[k][1:2]
    table = jnp.transpose(
        jnp.concatenate(facs + [jnp.broadcast_to(total, (8, 128))], axis=0)
    )
    x_acc.wait_all()
    merged = table[:lines, 0:1] * gacc[0].astype(f32)
    for k in range(1, n):
        merged = merged + table[:lines, k : k + 1] * gacc[k].astype(f32)
    ratio = merged / table[:lines, n : n + 1]
    normed = []
    for g in range(kv_heads):
        base = g * 2 * half
        head = ratio[base : base + half] - lam[g * half : (g + 1) * half] * ratio[base + half : base + 2 * half]
        mean_sq = jnp.mean(head * head, axis=1, keepdims=True)
        normed.append(head * lax.rsqrt(mean_sq + 1.0 / ctx_total) * hg_v[...])
    mine_n[...] = jnp.concatenate(normed, axis=0).astype(bf16)
    x_n = ex("kv", 7, lambda p: mine_n, lambda p: all_n.at[p])
    x_n.start_all()
    all_n[me] = mine_n[...]
    x_n.wait_all()

    for b in range(B):
        norm_f[b * heads : (b + 1) * heads, :] = all_n[b].astype(f32)
    normed = jnp.concatenate(
        [norm_f[pl.ds(h, B, stride=heads), :].astype(bf16) for h in range(heads)], axis=1
    )
    attn_out = jnp.dot(normed, wo_v[...], preferred_element_type=f32)
    res_v[...] = (tok_v[...].astype(f32) + attn_out).astype(bf16)
    x_res = ex("tp", 0, lambda p: res_v, lambda p: all_res.at[p])
    x_res.start_all()
    all_res[my_tp] = res_v[...]
    x_res.wait_all()

    every = all_res[...].reshape(all_rows, cols).astype(f32)
    gained = (every * mg_v[...]).astype(bf16)
    row_sq = jnp.sum(every * every, axis=1, keepdims=True)
    square = lax.broadcasted_iota(jnp.int32, (all_rows, all_rows), 0) == lax.broadcasted_iota(
        jnp.int32, (all_rows, all_rows), 1
    )
    sq_v[...] = jnp.sum(jnp.where(square, row_sq, 0.0), axis=0, keepdims=True)
    x_sq = ex("kv", 8, lambda p: sq_v, lambda p: got_sq.at[p])
    x_sq.start_all()
    got_sq[me] = sq_v[...]
    cw = up_v.shape[2]

    def chunk(ref, c):
        return ref.at[pl.ds(c * R, R)]

    x_up = [
        Exchange(
            "kv",
            n,
            me,
            lambda p, c=c: up_v.at[p, pl.ds(c * R, R)],
            lambda p, c=c: got_up.at[p, pl.ds(c * R, R)],
            sems_up.at[0, c],
            sems_up.at[1, c],
        )
        for c in range(CHUNKS)
    ]
    x_act = [
        Exchange(
            "kv",
            n,
            me,
            lambda p, c=c: mine_act.at[pl.ds(c * R, R)],
            lambda p, c=c: all_act.at[p, pl.ds(c * R, R)],
            sems_up.at[2, c],
            sems_up.at[3, c],
        )
        for c in range(CHUNKS)
    ]

    def up_of(peer):
        w = wu_v[:, rows_of(peer * cw, cw)]
        return jnp.dot(gained, w, preferred_element_type=f32).astype(bf16)

    def up_step(k, carry):
        peer = lax.rem(me + k, n)
        up_v[peer] = up_of(peer)
        x_up[0].copy(peer).start()
        return carry

    lax.fori_loop(1, n, up_step, 0)
    for c in range(1, CHUNKS):
        x_up[c].start_all()
    got_up[me] = up_of(me)
    x_sq.wait_all()
    total = got_sq[0]
    for k in range(1, n):
        total = total + got_sq[k]
    inv_row = lax.rsqrt(total / full_width + norm_eps)
    inv_two = jnp.sum(jnp.where(square, inv_row, 0.0), axis=1, keepdims=True)
    for c in range(CHUNKS):
        at = pl.ds(c * R, R)
        x_up[c].wait_all()
        total = got_up[0, at].astype(f32)
        for k in range(1, n):
            total = total + got_up[k, at].astype(f32)
        pre = jnp.maximum(total * inv_two[c * R : (c + 1) * R], 0.0)
        mine_act[at, :] = (pre * pre).astype(bf16)
        x_act[c].start_all()
        all_act[me, at] = mine_act[at, :]

    x_down = ex("tp", 1, lambda p: down_v.at[rows_of(p * B, B)], lambda p: got_down.at[p])
    for c in range(CHUNKS):
        at = pl.ds(c * R, R)
        x_act[c].wait_all()
        act = jnp.concatenate([all_act[k, at] for k in range(n)], axis=1)
        down_v[at, :] = jnp.dot(act, wd_v[...], preferred_element_type=f32).astype(bf16)
        for p in range(c * R // B, (c + 1) * R // B):

            @pl.when(my_tp != p)
            def _(p=p):
                x_down.copy(p).start()

    got_down[my_tp] = down_v[rows_of(my_tp * B, B), :]
    x_down.wait_all()
    total = got_down[0].astype(f32)
    for k in range(1, n_tp):
        total = total + got_down[k].astype(f32)
    mixed[...] = (res_v[...].astype(f32) + total).astype(bf16)

    x_kv2.wait_all()
    for x in [x_s, x_q, x_kv, x_q2, x_kv2, x_acc, x_stat, x_n, x_res, x_sq, x_down] + x_up + x_act:
        x.drain()


def shards(
    tokens,
    cache_keys,
    cache_values,
    attn_gain,
    w_query,
    w_key,
    w_value,
    lambdas,
    head_gain,
    w_out,
    mlp_gain,
    w_up,
    w_down,
):
    B, tok_width = tokens.shape
    n = lax.axis_size("kv")
    n_tp = lax.axis_size("tp")
    kv_heads = cache_keys.shape[2]
    comp = cache_keys.shape[3] // 2
    vd = cache_values.shape[3]
    ctx = cache_keys.shape[1]
    heads = lambdas.shape[0]
    span = ctx * kv_heads
    all_rows = B * n_tp
    hidden = w_up.shape[1]
    cw = hidden // n
    lines = 2 * heads
    assert B == n and comp * 2 == 128 and vd == 128
    V = pltpu.VMEM
    scratch = [
        V(tokens.shape, bf16),
        V((1, tok_width), f32),
        V(w_query.shape, bf16),
        V(w_key.shape, bf16),
        V(w_value.shape, bf16),
        V((1, heads), f32),
        V((1, vd), f32),
        V((1, tok_width), f32),
        V((B, span, 128), bf16),
        V((B, span, 128), bf16),
        V(w_out.shape, bf16),
        V(w_up.shape, bf16),
        V(w_down.shape, bf16),
        DMA((11,)),
        DMA((B,)),
        DMA((B,)),
        V((B * heads, 128), f32),
        V((B, 1, 128), f32),
        V((B * 8, 128), f32),
        V((n, heads, 128), f32),
        V((n, 1, 128), f32),
        V((n, 8, 128), f32),
        V((heads, 128), bf16),
        V((8, 128), bf16),
        V((n, heads, 128), bf16),
        V((n, lines, vd), bf16),
        V((n, 2, 128), f32),
        V((n, lines, vd), bf16),
        V((n, 2, 128), f32),
        V((heads, vd), bf16),
        V((n, heads, vd), bf16),
        V((B * heads, vd), f32),
        V((B, tok_width), bf16),
        V((n_tp, B, tok_width), bf16),
        V((1, all_rows), f32),
        V((n, 1, all_rows), f32),
        V((n, all_rows, cw), bf16),
        V((n, all_rows, cw), bf16),
        V((all_rows, cw), bf16),
        V((n, all_rows, cw), bf16),
        V((all_rows, tok_width), bf16),
        V((n_tp, B, tok_width), bf16),
        DMA((18, n)),
        DMA((4, n_tp)),
        DMA((4, CHUNKS, n)),
    ]
    mixed, kv_out = pl.pallas_call(
        functools.partial(
            layer_kernel, n, n_tp, kv_heads, tok_width * n, ctx * n, comp ** (-0.5)
        ),
        out_shape=(
            jax.ShapeDtypeStruct((B, tok_width), bf16),
            jax.ShapeDtypeStruct((n, 8, 128), bf16),
        ),
        in_specs=[ANY] * 13,
        out_specs=(VM, VM),
        scratch_shapes=scratch,
        compiler_params=pltpu.CompilerParams(
            collective_id=0, has_side_effects=True, vmem_limit_bytes=60 * 1024 * 1024
        ),
    )(
        tokens,
        cache_keys.reshape(B, span, 128),
        cache_values.reshape(B, span, vd),
        attn_gain.reshape(1, tok_width),
        w_query,
        w_key,
        w_value,
        lambdas.reshape(1, heads),
        head_gain.reshape(1, vd),
        w_out,
        mlp_gain.reshape(1, tok_width),
        w_up,
        w_down,
    )
    return mixed, kv_out[:, :kv_heads], kv_out[:, kv_heads : 2 * kv_heads]


def solution(mesh):
    in_specs = (
        P("tp", "kv"),
        P("tp", "kv", None, None),
        P("tp", "kv", None, None),
        P("kv"),
        P("kv", None),
        P("kv", None),
        P("kv", None),
        P(),
        P(),
        P(None, "kv"),
        P("kv"),
        P("kv", "tp"),
        P("tp", "kv"),
    )
    out_specs = (P("tp", "kv"), P("tp", None, None), P("tp", None, None))
    return jax.shard_map(shards, mesh=mesh, in_specs=in_specs, out_specs=out_specs, check_vma=False)
```

time: 96.8 us -> 67.6 us (0.70)
  blocking collectives: 17.8 us -> 0 us
  matrix products: 4.56 us -> 0 us
  Pallas kernels: 68.1 us -> 63.9 us
  local copies, waits for them, and re-layouts: 3.93 us -> 2.74 us
  other arithmetic: 1.05 us -> 0 us
    all_gather x1 -> x0, blocking collectives: 17.8 us -> none  [shards(): everyone = lax.all_gather(residual, 'tp', axis=0, tiled=True)]
    dot_general x6 -> x0, matrix products: 4.56 us -> none  [the longest x3 3.68 us: shards(): jnp.dot(scaled, w, preferred_element_type=f32)]
    pallas_call x4 -> x1, Pallas kernels: 68.1 us -> 63.9 us  [shards(): pl.pallas_call(functools.partial(layer_kernel, n, n_tp, kv_heads, tok_wid...]
    broadcast_in_dim x4 -> x0, local copies, waits for them, and re-layouts: 1.46 us -> none  [the longest x1 0.73 us: shards(): lam = jnp.broadcast_to(lambdas[:, None], (heads, 128))]
    reshape x3 -> x0, local copies, waits for them, and re-layouts: 1.34 us -> none  [the longest x1 0.61 us: shards(): new_values = proj[:, qw + kw:].reshape(B, kv_heads, vd)]
    slice x2 -> x1, local copies, waits for them, and re-layouts: 0.19 us -> 1.45 us  [shards(): return (mixed, kv_out[:, :kv_heads], kv_out[:, kv_heads:2 * kv_heads])]
    reduce_sum x2 -> x0, other arithmetic: 1 us -> none  [the longest x1 0.9 us: shards(): squares = jnp.sum(tok_f * tok_f, axis=1, keepdims=True)]
where the time goes in v1:
time: 67.6 us; the launch traced here: 67.3 us
  Pallas kernels  63.9 us (95%)
  local copies, waits for them, and re-layouts  2.74 us (4%)
    pallas_call x1, Pallas kernels, shards(): pl.pallas_call(functools.partial(layer_kernel, n, n_tp, kv_heads, tok_wid...  63.9 us
    slice x1, local copies, waits for them, and re-layouts, shards(): return (mixed, kv_out[:, :kv_heads], kv_out[:, kv_heads:2 * kv_heads])  1.45 us

profile of v1, /device:TPU:1, one launch (start us, length us, event | category | flops | bytes accessed | tf_op | source)
XLA Modules:
  0.0 67.3 jit_solution(12667399726855567830)
XLA Ops:
  0.6 63.9 %shard_map.148 = (bf16[16,256]{1,0:T(8,128)(2,1)}, bf16[16,8,128]{2,1,0:T(8,128)(2,1)}) custom-call(bf16[16,256]{1,0:T(8,128)(2,1)} %tokens.1, bf16[16,2048,128]{2,1,0:T(8,128)(2,1)} %bitcast.6, bf16[16,2048,128]{2,1,0:T(8,128)(2,1)} %bitcast.7, f32[1,256]{1,0:T(1,128)} %bitcast.8, bf16[256,2048]{1,0:T(8,128)(2,1)} %w_query.1, bf16[256,256]{1,0:T(8,128)(2,1)} %w_key.1, ...), custom_call_target="tpu_custom_call" | custom-call | tf_op jit(solution)/shard_map/pallas_call | solution.py:552
  64.6 1.4 %fusion = (bf16[16,2,128]{2,1,0:T(2,128)(2,1)}, bf16[16,2,128]{2,1,0:T(2,128)(2,1)}) fusion(bf16[16,8,128]{2,1,0:T(8,128)(2,1)} %get-tuple-element.6), kind=kLoop, calls=%fused_computation | loop fusion | bytes 32768 | tf_op jit(solution)/shard_map/slice | solution.py:581
  66.0 1.3 %copy.17 = bf16[16,256]{1,0:T(8,128)(2,1)} copy(bf16[16,256]{1,0:T(8,128)(2,1)} %get-tuple-element.12) | data formatting | bytes 16384

commit v2 on v1

--- a/solution.py
+++ b/solution.py
@@ -11,7 +11,7 @@
 f32 = jnp.float32
 bf16 = jnp.bfloat16
 VM = pl.BlockSpec(memory_space=pltpu.VMEM)
-ANY = pl.BlockSpec(memory_space=pl.ANY)
+HBM = pl.BlockSpec(memory_space=pltpu.HBM)
 DMA = pltpu.SemaphoreType.DMA
 NT = (((1,), (1,)), ((), ()))
 CHUNKS = 2
@@ -30,14 +30,14 @@
 
 
 class Exchange:
-    def __init__(self, axis, n, me, src_of, dst_of, send, recv):
+    def __init__(self, axis, n, me, src_of, dst_of, all_dst, sems):
         self.axis, self.n, self.me = axis, n, me
-        self.src_of, self.dst_of, self.send, self.recv = src_of, dst_of, send, recv
+        self.src_of, self.dst_of, self.all_dst = src_of, dst_of, all_dst
+        self.send, self.recv = sems.at[0], sems.at[1]
 
     def copy(self, peer):
-        me = self.me
         return remote(
-            self.src_of(peer), self.dst_of(me), self.send.at[peer], self.recv.at[me], self.axis, peer
+            self.src_of(peer), self.dst_of(self.me), self.send, self.recv, self.axis, peer
         )
 
     def start(self, k):
@@ -47,18 +47,15 @@
         for k in range(1, self.n):
             self.start(k)
 
-    def wait_from(self, peer):
-        remote(
-            self.src_of(peer), self.dst_of(peer), self.send.at[peer], self.recv.at[peer], self.axis, peer
-        ).wait_recv()
+    def everything(self):
+        other = lax.rem(self.me + 1, self.n)
+        return remote(self.all_dst, self.all_dst, self.send, self.recv, self.axis, other)
 
     def wait_all(self):
-        for k in range(1, self.n):
-            self.wait_from(lax.rem(self.me + self.n - k, self.n))
+        self.everything().wait_recv()
 
     def drain(self):
-        for k in range(1, self.n):
-            self.copy(lax.rem(self.me + k, self.n)).wait_send()
+        self.everything().wait_send()
 
 
 def rows_of(start, size):
@@ -129,9 +126,7 @@
     all_act,
     down_v,
     got_down,
-    sems16,
-    sems8,
-    sems_up,
+    sems,
 ):
     me = lax.axis_index("kv")
     my_tp = lax.axis_index("tp")
@@ -145,10 +140,11 @@
     R = all_rows // CHUNKS
     groups = span // 128
 
-    def ex(axis, i, src_of, dst_of):
-        if axis == "kv":
-            return Exchange("kv", n, me, src_of, dst_of, sems16.at[2 * i], sems16.at[2 * i + 1])
-        return Exchange("tp", n_tp, my_tp, src_of, dst_of, sems8.at[2 * i], sems8.at[2 * i + 1])
+    def ex(axis, i, src_of, dst):
+        size, at = (n, me) if axis == "kv" else (n_tp, my_tp)
+        return Exchange(
+            axis, size, at, src_of, lambda p: dst.at[p], dst.at[pl.ds(0, size - 1)], sems.at[i]
+        )
 
     first = [(tokens, tok_v), (attn_gain, ag_v), (w_query, wq_v), (w_key, wk_v), (w_value, wv_v)]
     later = [
@@ -177,8 +173,8 @@
 
     def fetch(b):
         return (
-            pltpu.make_async_copy(keys.at[b], kbuf.at[b], ksem.at[b]),
-            pltpu.make_async_copy(values.at[b], vbuf.at[b], vsem.at[b]),
+            pltpu.make_async_copy(keys.at[b], kbuf.at[b], ksem),
+            pltpu.make_async_copy(values.at[b], vbuf.at[b], vsem),
         )
 
     def fetch_step(j, carry):
@@ -207,9 +203,9 @@
     for h in range(pieces, 8):
         part_kv[pl.ds(h, B, stride=8), :] = jnp.zeros((B, 128), f32)
 
-    x_q = ex("kv", 0, lambda p: part_q.at[rows_of(p * heads, heads)], lambda p: got_q.at[p])
-    x_s = ex("kv", 1, lambda p: part_s.at[p], lambda p: got_s.at[p])
-    x_kv = ex("kv", 2, lambda p: part_kv.at[rows_of(p * 8, 8)], lambda p: got_kv.at[p])
+    x_q = ex("kv", 0, lambda p: part_q.at[rows_of(p * heads, heads)], got_q)
+    x_s = ex("kv", 1, lambda p: part_s.at[p], got_s)
+    x_kv = ex("kv", 2, lambda p: part_kv.at[rows_of(p * 8, 8)], got_kv)
     pl.semaphore_wait(barrier, n - 1 + n_tp - 1)
     for k in range(1, n):
         x_s.start(k)
@@ -229,15 +225,17 @@
         total = total + got_q[k]
     query = (total * inv_one).astype(bf16).astype(f32) * scale
     mine_q[...] = query.astype(bf16)
-    x_q2 = ex("kv", 3, lambda p: mine_q, lambda p: all_q.at[p])
+    x_q2 = ex("kv", 3, lambda p: mine_q, all_q)
     x_q2.start_all()
     all_q[me] = mine_q[...]
     x_kv.wait_all()
     total = got_kv[0]
     for k in range(1, n):
         total = total + got_kv[k]
-    mine_kv[...] = (total * inv_one).astype(bf16)
-    x_kv2 = ex("kv", 4, lambda p: mine_kv, lambda p: kv_out.at[p])
+    new_kv = (total * inv_one).astype(bf16)
+    for i in range(2):
+        mine_kv[i] = new_kv[i * kv_heads : (i + 1) * kv_heads]
+    x_kv2 = ex("kv", 4, lambda p: mine_kv, kv_out)
     x_kv2.start_all()
     kv_out[me] = mine_kv[...]
 
@@ -248,8 +246,8 @@
         jnp.int32, (lines, 128), 0
     )
 
-    x_acc = ex("kv", 5, lambda p: acc.at[p], lambda p: gacc.at[p])
-    x_stat = ex("kv", 6, lambda p: stat.at[p], lambda p: gstat.at[p])
+    x_acc = ex("kv", 5, lambda p: acc.at[p], gacc)
+    x_stat = ex("kv", 6, lambda p: stat.at[p], gstat)
 
     def dest(j):
         return lax.rem(me + 1 + j, n)
@@ -292,17 +290,6 @@
 
     def step(i, carry):
         bs = [dest(i * UNROLL + u) for u in range(UNROLL)]
-        for u, b in enumerate(bs):
-            if u == UNROLL - 1:
-
-                @pl.when(b != me)
-                def _(b=b):
-                    x_q2.wait_from(b)
-
-            else:
-                x_q2.wait_from(b)
-            for c in fetch(b):
-                c.wait()
         results = [one_row(b) for b in bs]
         for u, (b, (o, st)) in enumerate(zip(bs, results)):
             acc[b] = o
@@ -320,6 +307,9 @@
                 x_stat.copy(b).start()
         return carry
 
+    x_q2.wait_all()
+    pltpu.make_async_copy(keys, kbuf, ksem).wait()
+    pltpu.make_async_copy(values, vbuf, vsem).wait()
     lax.fori_loop(0, B // UNROLL, step, 0)
     gacc[me] = acc[me]
     gstat[me] = stat[me]
@@ -360,7 +350,7 @@
         mean_sq = jnp.mean(head * head, axis=1, keepdims=True)
         normed.append(head * lax.rsqrt(mean_sq + 1.0 / ctx_total) * hg_v[...])
     mine_n[...] = jnp.concatenate(normed, axis=0).astype(bf16)
-    x_n = ex("kv", 7, lambda p: mine_n, lambda p: all_n.at[p])
+    x_n = ex("kv", 7, lambda p: mine_n, all_n)
     x_n.start_all()
     all_n[me] = mine_n[...]
     x_n.wait_all()
@@ -372,7 +362,7 @@
     )
     attn_out = jnp.dot(normed, wo_v[...], preferred_element_type=f32)
     res_v[...] = (tok_v[...].astype(f32) + attn_out).astype(bf16)
-    x_res = ex("tp", 0, lambda p: res_v, lambda p: all_res.at[p])
+    x_res = ex("tp", 9, lambda p: res_v, all_res)
     x_res.start_all()
     all_res[my_tp] = res_v[...]
     x_res.wait_all()
@@ -384,38 +374,29 @@
         jnp.int32, (all_rows, all_rows), 1
     )
     sq_v[...] = jnp.sum(jnp.where(square, row_sq, 0.0), axis=0, keepdims=True)
-    x_sq = ex("kv", 8, lambda p: sq_v, lambda p: got_sq.at[p])
+    x_sq = ex("kv", 8, lambda p: sq_v, got_sq)
     x_sq.start_all()
     got_sq[me] = sq_v[...]
     cw = up_v.shape[2]
 
-    def chunk(ref, c):
-        return ref.at[pl.ds(c * R, R)]
-
-    x_up = [
-        Exchange(
-            "kv",
-            n,
-            me,
-            lambda p, c=c: up_v.at[p, pl.ds(c * R, R)],
-            lambda p, c=c: got_up.at[p, pl.ds(c * R, R)],
-            sems_up.at[0, c],
-            sems_up.at[1, c],
-        )
-        for c in range(CHUNKS)
-    ]
-    x_act = [
-        Exchange(
-            "kv",
-            n,
-            me,
-            lambda p, c=c: mine_act.at[pl.ds(c * R, R)],
-            lambda p, c=c: all_act.at[p, pl.ds(c * R, R)],
-            sems_up.at[2, c],
-            sems_up.at[3, c],
-        )
-        for c in range(CHUNKS)
-    ]
+    x_up, x_act = [], []
+    for c in range(CHUNKS):
+        at = pl.ds(c * R, R)
+        for xs, src_of, dst, i in (
+            (x_up, lambda p, at=at: up_v.at[p, at], got_up, 11 + 2 * c),
+            (x_act, lambda p, at=at: mine_act.at[at], all_act, 12 + 2 * c),
+        ):
+            xs.append(
+                Exchange(
+                    "kv",
+                    n,
+                    me,
+                    src_of,
+                    lambda p, dst=dst, at=at: dst.at[p, at],
+                    dst.at[pl.ds(0, n - 1), at],
+                    sems.at[i],
+                )
+            )
 
     def up_of(peer):
         w = wu_v[:, rows_of(peer * cw, cw)]
@@ -448,7 +429,7 @@
         x_act[c].start_all()
         all_act[me, at] = mine_act[at, :]
 
-    x_down = ex("tp", 1, lambda p: down_v.at[rows_of(p * B, B)], lambda p: got_down.at[p])
+    x_down = ex("tp", 10, lambda p: down_v.at[rows_of(p * B, B)], got_down)
     for c in range(CHUNKS):
         at = pl.ds(c * R, R)
         x_act[c].wait_all()
@@ -470,6 +451,19 @@
     x_kv2.wait_all()
     for x in [x_s, x_q, x_kv, x_q2, x_kv2, x_acc, x_stat, x_n, x_res, x_sq, x_down] + x_up + x_act:
         x.drain()
+
+
+def result_kernel(mixed, kv_out, out, new_keys, new_values, sems):
+    copies = [
+        pltpu.make_async_copy(src, dst, sems.at[i])
+        for i, (src, dst) in enumerate(
+            ((mixed, out), (kv_out.at[:, 0], new_keys), (kv_out.at[:, 1], new_values))
+        )
+    ]
+    for c in copies:
+        c.start()
+    for c in copies:
+        c.wait()
 
 
 def shards(
@@ -517,8 +511,8 @@
         V(w_up.shape, bf16),
         V(w_down.shape, bf16),
         DMA((11,)),
-        DMA((B,)),
-        DMA((B,)),
+        DMA,
+        DMA,
         V((B * heads, 128), f32),
         V((B, 1, 128), f32),
         V((B * 8, 128), f32),
@@ -526,7 +520,7 @@
         V((n, 1, 128), f32),
         V((n, 8, 128), f32),
         V((heads, 128), bf16),
-        V((8, 128), bf16),
+        V((2, kv_heads, 128), bf16),
         V((n, heads, 128), bf16),
         V((n, lines, vd), bf16),
         V((n, 2, 128), f32),
@@ -545,9 +539,7 @@
         V((n, all_rows, cw), bf16),
         V((all_rows, tok_width), bf16),
         V((n_tp, B, tok_width), bf16),
-        DMA((18, n)),
-        DMA((4, n_tp)),
-        DMA((4, CHUNKS, n)),
+        DMA((11 + 2 * CHUNKS, 2)),
     ]
     mixed, kv_out = pl.pallas_call(
         functools.partial(
@@ -555,30 +547,46 @@
         ),
         out_shape=(
             jax.ShapeDtypeStruct((B, tok_width), bf16),
-            jax.ShapeDtypeStruct((n, 8, 128), bf16),
+            jax.ShapeDtypeStruct((n, 2, kv_heads, 128), bf16),
         ),
-        in_specs=[ANY] * 13,
+        in_specs=[HBM] * 13,
         out_specs=(VM, VM),
         scratch_shapes=scratch,
         compiler_params=pltpu.CompilerParams(
-            collective_id=0, has_side_effects=True, vmem_limit_bytes=60 * 1024 * 1024
+            collective_id=0, has_side_effects=True, vmem_limit_bytes=48 * 1024 * 1024
         ),
     )(
-        tokens,
-        cache_keys.reshape(B, span, 128),
-        cache_values.reshape(B, span, vd),
-        attn_gain.reshape(1, tok_width),
-        w_query,
-        w_key,
-        w_value,
-        lambdas.reshape(1, heads),
-        head_gain.reshape(1, vd),
-        w_out,
-        mlp_gain.reshape(1, tok_width),
-        w_up,
-        w_down,
-    )
-    return mixed, kv_out[:, :kv_heads], kv_out[:, kv_heads : 2 * kv_heads]
+        *[
+            pltpu.with_memory_space_constraint(x, pltpu.HBM)
+            for x in (
+                tokens,
+                cache_keys.reshape(B, span, 128),
+                cache_values.reshape(B, span, vd),
+                attn_gain.reshape(1, tok_width),
+                w_query,
+                w_key,
+                w_value,
+                lambdas.reshape(1, heads),
+                head_gain.reshape(1, vd),
+                w_out,
+                mlp_gain.reshape(1, tok_width),
+                w_up,
+                w_down,
+            )
+        ]
+    )
+    return pl.pallas_call(
+        result_kernel,
+        out_shape=(
+            jax.ShapeDtypeStruct(mixed.shape, bf16),
+            jax.ShapeDtypeStruct((n, kv_heads, 128), bf16),
+            jax.ShapeDtypeStruct((n, kv_heads, 128), bf16),
+        ),
+        in_specs=[VM, VM],
+        out_specs=(HBM, HBM, HBM),
+        scratch_shapes=[DMA((3,))],
+        compiler_params=pltpu.CompilerParams(vmem_limit_bytes=1024 * 1024),
+    )(mixed, kv_out)
 
 
 def solution(mesh):

time: 67.6 us -> 61.1 us (0.904)
  Pallas kernels: 63.9 us -> 60.3 us
  local copies, waits for them, and re-layouts: 2.74 us -> 0 us
    pallas_call x1, Pallas kernels: 63.9 us -> 59.7 us  [shards(): pl.pallas_call(functools.partial(layer_kernel, n, n_tp, kv_heads, tok_wid...]
    slice x1 -> x0, local copies, waits for them, and re-layouts: 1.45 us -> none  [shards(): return (mixed, kv_out[:, :kv_heads], kv_out[:, kv_heads:2 * kv_heads])]
    unnamed x1 -> x0, local copies, waits for them, and re-layouts: 1.29 us -> none
where the time goes in v2:
time: 61.1 us; the launch traced here: 61 us
  Pallas kernels  60.3 us (99%)
  between operations  0.64 us (1%)
    pallas_call x1, Pallas kernels, shards(): pl.pallas_call(functools.partial(layer_kernel, n, n_tp, kv_heads, tok_wid...  59.7 us

profile of v2, /device:TPU:1, one launch (start us, length us, event | category | flops | bytes accessed | tf_op | source)
XLA Modules:
  0.0 61.0 jit_solution(14510741326224536047)
XLA Ops:
  0.6 59.7 %shard_map.148 = (bf16[16,256]{1,0:T(8,128)(2,1)S(1)}, bf16[16,2,2,128]{3,2,1,0:T(2,128)(2,1)S(1)}) custom-call(bf16[16,256]{1,0:T(8,128)(2,1)} %tokens.1, bf16[16,2048,128]{2,1,0:T(8,128)(2,1)} %bitcast.6, bf16[16,2048,128]{2,1,0:T(8,128)(2,1)} %bitcast.7, f32[1,256]{1,0:T(1,128)} %bitcast.8, bf16[256,2048]{1,0:T(8,128)(2,1)} %w_query.1, ...), custom_call_target="tpu_custom_call" | custom-call | tf_op jit(solution)/shard_map/pallas_call | solution.py:544
  60.3 0.6 %shard_map.149 = (bf16[16,256]{1,0:T(8,128)(2,1)}, bf16[16,2,128]{2,1,0:T(2,128)(2,1)}, bf16[16,2,128]{2,1,0:T(2,128)(2,1)}) custom-call(bf16[16,256]{1,0:T(8,128)(2,1)S(1)} %get-tuple-element.5.mixed, bf16[16,2,2,128]{3,2,1,0:T(2,128)(2,1)S(1)} %get-tuple-element.6.kv_out), custom_call_target="tpu_custom_call" | custom-call | tf_op jit(solution)/shard_map/pallas_call | solution.py:578

commit v3 on v2

--- a/solution.py
+++ b/solution.py
@@ -14,8 +14,7 @@
 HBM = pl.BlockSpec(memory_space=pltpu.HBM)
 DMA = pltpu.SemaphoreType.DMA
 NT = (((1,), (1,)), ((), ()))
-CHUNKS = 2
-UNROLL = 2
+UNROLL = 4
 
 
 def remote(src, dst, send, recv, axis, peer):
@@ -30,8 +29,8 @@
 
 
 class Exchange:
-    def __init__(self, axis, n, me, src_of, dst_of, all_dst, sems):
-        self.axis, self.n, self.me = axis, n, me
+    def __init__(self, axis, peers, me, src_of, dst_of, all_dst, sems):
+        self.axis, self.peers, self.me = axis, peers, me
         self.src_of, self.dst_of, self.all_dst = src_of, dst_of, all_dst
         self.send, self.recv = sems.at[0], sems.at[1]
 
@@ -40,22 +39,27 @@
             self.src_of(peer), self.dst_of(self.me), self.send, self.recv, self.axis, peer
         )
 
-    def start(self, k):
-        self.copy(lax.rem(self.me + k, self.n)).start()
-
     def start_all(self):
-        for k in range(1, self.n):
-            self.start(k)
+        for peer in self.peers:
+            self.copy(peer).start()
 
     def everything(self):
-        other = lax.rem(self.me + 1, self.n)
-        return remote(self.all_dst, self.all_dst, self.send, self.recv, self.axis, other)
+        return remote(self.all_dst, self.all_dst, self.send, self.recv, self.axis, self.peers[0])
 
     def wait_all(self):
         self.everything().wait_recv()
 
     def drain(self):
         self.everything().wait_send()
+
+
+def offsets(outer, inner, wrap_inner):
+    def far(d, size, wrap):
+        return min(d, size - d) if wrap else d % 2
+
+    every = [(a, b) for a in range(outer) for b in range(inner)]
+    every.sort(key=lambda o: -(far(o[0], outer, True) + far(o[1], inner, wrap_inner) / 1.5))
+    return every
 
 
 def rows_of(start, size):
@@ -127,6 +131,7 @@
     down_v,
     got_down,
     sems,
+    res_sem,
 ):
     me = lax.axis_index("kv")
     my_tp = lax.axis_index("tp")
@@ -137,13 +142,28 @@
     span = keys.shape[1]
     cols = tok_v.shape[1]
     all_rows = B * n_tp
-    R = all_rows // CHUNKS
+    R = 2 * B
     groups = span // 128
 
-    def ex(axis, i, src_of, dst):
-        size, at = (n, me) if axis == "kv" else (n_tp, my_tp)
+    def order(at, outer, inner, wrap_inner):
+        a, b = at // inner, lax.rem(at, inner)
+        return [
+            lax.rem(a + da, outer) * inner + lax.rem(b + db, inner)
+            for da, db in offsets(outer, inner, wrap_inner)
+        ]
+
+    side = int(n**0.5)
+    ny = n_tp // 2
+    kv_order = order(me, side, side, True)
+    kv_peers = kv_order[:-1]
+    near_peers, far_peers = kv_order[-5:-1], kv_order[:-5]
+    tp_peers = order(my_tp, ny, 2, False)[:-1]
+
+    def ex(axis, i, src_of, dst, peers=None):
+        every, at = (kv_peers, me) if axis == "kv" else (tp_peers, my_tp)
+        peers = every if peers is None else peers
         return Exchange(
-            axis, size, at, src_of, lambda p: dst.at[p], dst.at[pl.ds(0, size - 1)], sems.at[i]
+            axis, peers, at, src_of, lambda p: dst.at[p], dst.at[pl.ds(0, len(peers))], sems.at[i]
         )
 
     first = [(tokens, tok_v), (attn_gain, ag_v), (w_query, wq_v), (w_key, wk_v), (w_value, wv_v)]
@@ -160,13 +180,10 @@
     for c in first:
         c.start()
     barrier = pltpu.get_barrier_semaphore()
-    for axis, size, at in (("kv", n, me), ("tp", n_tp, my_tp)):
-        for k in range(1, size):
+    for axis, peers in (("kv", kv_peers), ("tp", tp_peers)):
+        for peer in peers:
             pl.semaphore_signal(
-                barrier,
-                inc=1,
-                device_id={axis: lax.rem(at + k, size)},
-                device_id_type=pl.DeviceIdType.MESH,
+                barrier, inc=1, device_id={axis: peer}, device_id_type=pl.DeviceIdType.MESH
             )
     for c in first:
         c.wait()
@@ -177,12 +194,9 @@
             pltpu.make_async_copy(values.at[b], vbuf.at[b], vsem),
         )
 
-    def fetch_step(j, carry):
-        for c in fetch(lax.rem(me + 1 + j, n)):
+    for b in kv_order:
+        for c in fetch(b):
             c.start()
-        return carry
-
-    lax.fori_loop(0, B, fetch_step, 0)
     for c in later:
         c.start()
 
@@ -207,9 +221,9 @@
     x_s = ex("kv", 1, lambda p: part_s.at[p], got_s)
     x_kv = ex("kv", 2, lambda p: part_kv.at[rows_of(p * 8, 8)], got_kv)
     pl.semaphore_wait(barrier, n - 1 + n_tp - 1)
-    for k in range(1, n):
-        x_s.start(k)
-        x_q.start(k)
+    for peer in kv_peers:
+        x_s.copy(peer).start()
+        x_q.copy(peer).start()
     x_kv.start_all()
     got_q[me] = part_q[rows_of(me * heads, heads), :]
     got_s[me] = part_s[me]
@@ -225,8 +239,10 @@
         total = total + got_q[k]
     query = (total * inv_one).astype(bf16).astype(f32) * scale
     mine_q[...] = query.astype(bf16)
-    x_q2 = ex("kv", 3, lambda p: mine_q, all_q)
-    x_q2.start_all()
+    x_far = ex("kv", 3, lambda p: mine_q, all_q, far_peers)
+    x_near = ex("kv", 8, lambda p: mine_q, all_q, near_peers)
+    x_far.start_all()
+    x_near.start_all()
     all_q[me] = mine_q[...]
     x_kv.wait_all()
     total = got_kv[0]
@@ -248,9 +264,6 @@
 
     x_acc = ex("kv", 5, lambda p: acc.at[p], gacc)
     x_stat = ex("kv", 6, lambda p: stat.at[p], gstat)
-
-    def dest(j):
-        return lax.rem(me + 1 + j, n)
 
     def one_row(b):
         q = all_q[b].astype(f32)
@@ -288,29 +301,22 @@
         row1 = jnp.sum(jnp.where(diag, tots, 0.0), axis=0, keepdims=True)
         return o.astype(bf16), jnp.concatenate([row0, row1], axis=0)
 
-    def step(i, carry):
-        bs = [dest(i * UNROLL + u) for u in range(UNROLL)]
-        results = [one_row(b) for b in bs]
-        for u, (b, (o, st)) in enumerate(zip(bs, results)):
+    def attend(bs, send=True):
+        for b, (o, st) in zip(bs, [one_row(b) for b in bs]):
             acc[b] = o
             stat[b] = st
-        for u, b in enumerate(bs):
-            if u == UNROLL - 1:
-
-                @pl.when(b != me)
-                def _(b=b):
-                    x_acc.copy(b).start()
-                    x_stat.copy(b).start()
-
-            else:
-                x_acc.copy(b).start()
-                x_stat.copy(b).start()
-        return carry
-
-    x_q2.wait_all()
+        for b in bs if send else ():
+            x_acc.copy(b).start()
+            x_stat.copy(b).start()
+
     pltpu.make_async_copy(keys, kbuf, ksem).wait()
     pltpu.make_async_copy(values, vbuf, vsem).wait()
-    lax.fori_loop(0, B // UNROLL, step, 0)
+    attend([me], send=False)
+    x_near.wait_all()
+    attend(near_peers)
+    x_far.wait_all()
+    for i in range(0, len(far_peers), UNROLL):
+        attend(far_peers[i : i + UNROLL])
     gacc[me] = acc[me]
     gstat[me] = stat[me]
     for c in later:
@@ -362,34 +368,44 @@
     )
     attn_out = jnp.dot(normed, wo_v[...], preferred_element_type=f32)
     res_v[...] = (tok_v[...].astype(f32) + attn_out).astype(bf16)
-    x_res = ex("tp", 9, lambda p: res_v, all_res)
-    x_res.start_all()
+    my_y, my_c = my_tp // 2, lax.rem(my_tp, 2)
+    res_sent = sems.at[9, 0]
+
+    def res_copy(dy, dc):
+        peer = lax.rem(my_y + dy, ny) * 2 + lax.rem(my_c + dc, 2)
+        return remote(res_v, all_res.at[my_tp], res_sent, res_sem.at[(ny - dy) % ny], "tp", peer)
+
+    for dy, dc in [(0, 1)] + [(d, c) for d in range(ny - 1, 0, -1) for c in range(2)]:
+        res_copy(dy, dc).start()
     all_res[my_tp] = res_v[...]
-    x_res.wait_all()
-
-    every = all_res[...].reshape(all_rows, cols).astype(f32)
-    gained = (every * mg_v[...]).astype(bf16)
-    row_sq = jnp.sum(every * every, axis=1, keepdims=True)
-    square = lax.broadcasted_iota(jnp.int32, (all_rows, all_rows), 0) == lax.broadcasted_iota(
-        jnp.int32, (all_rows, all_rows), 1
-    )
-    sq_v[...] = jnp.sum(jnp.where(square, row_sq, 0.0), axis=0, keepdims=True)
-    x_sq = ex("kv", 8, lambda p: sq_v, got_sq)
-    x_sq.start_all()
-    got_sq[me] = sq_v[...]
+
     cw = up_v.shape[2]
-
-    x_up, x_act = [], []
-    for c in range(CHUNKS):
-        at = pl.ds(c * R, R)
+    square = lax.broadcasted_iota(jnp.int32, (R, 128), 0) == lax.broadcasted_iota(
+        jnp.int32, (R, 128), 1
+    )
+    chips = [lax.rem(my_y + dy, ny) for dy in range(ny)]
+    ats = [rows_of(y * R, R) for y in chips]
+    x_sq, x_up, x_act = [], [], []
+    for dy, at in enumerate(ats):
+        x_sq.append(
+            Exchange(
+                "kv",
+                kv_peers,
+                me,
+                lambda p, dy=dy: sq_v.at[dy],
+                lambda p, dy=dy: got_sq.at[dy, p],
+                got_sq.at[dy, pl.ds(0, n - 1)],
+                sems.at[11 + 3 * dy],
+            )
+        )
         for xs, src_of, dst, i in (
-            (x_up, lambda p, at=at: up_v.at[p, at], got_up, 11 + 2 * c),
-            (x_act, lambda p, at=at: mine_act.at[at], all_act, 12 + 2 * c),
+            (x_up, lambda p, at=at: up_v.at[p, at], got_up, 12 + 3 * dy),
+            (x_act, lambda p, at=at: mine_act.at[at], all_act, 13 + 3 * dy),
         ):
             xs.append(
                 Exchange(
                     "kv",
-                    n,
+                    kv_peers,
                     me,
                     src_of,
                     lambda p, dst=dst, at=at: dst.at[p, at],
@@ -398,49 +414,44 @@
                 )
             )
 
-    def up_of(peer):
-        w = wu_v[:, rows_of(peer * cw, cw)]
-        return jnp.dot(gained, w, preferred_element_type=f32).astype(bf16)
-
-    def up_step(k, carry):
-        peer = lax.rem(me + k, n)
-        up_v[peer] = up_of(peer)
-        x_up[0].copy(peer).start()
-        return carry
-
-    lax.fori_loop(1, n, up_step, 0)
-    for c in range(1, CHUNKS):
-        x_up[c].start_all()
-    got_up[me] = up_of(me)
-    x_sq.wait_all()
-    total = got_sq[0]
-    for k in range(1, n):
-        total = total + got_sq[k]
-    inv_row = lax.rsqrt(total / full_width + norm_eps)
-    inv_two = jnp.sum(jnp.where(square, inv_row, 0.0), axis=1, keepdims=True)
-    for c in range(CHUNKS):
-        at = pl.ds(c * R, R)
-        x_up[c].wait_all()
+    for dy, (y, at) in enumerate(zip(chips, ats)):
+        arrived = all_res.at[pl.ds(0, 2 if dy else 1)]
+        remote(arrived, arrived, res_sent, res_sem.at[dy], "tp", tp_peers[0]).wait_recv()
+        every = all_res[pl.ds(y * 2, 2)].reshape(R, cols).astype(f32)
+        gained = (every * mg_v[...]).astype(bf16)
+        row_sq = jnp.sum(every * every, axis=1, keepdims=True)
+        sq_v[dy] = jnp.sum(jnp.where(square, row_sq, 0.0), axis=0, keepdims=True)
+        up = jnp.dot(gained, wu_v[...], preferred_element_type=f32)
+        for p in range(n):
+            up_v[p, at] = up[:, p * cw : (p + 1) * cw].astype(bf16)
+        for peer in kv_peers:
+            x_sq[dy].copy(peer).start()
+            x_up[dy].copy(peer).start()
+        got_sq[dy, me] = sq_v[dy]
+        got_up[me, at] = up_v[me, at]
+    for dy, at in enumerate(ats):
+        x_sq[dy].wait_all()
+        total = got_sq[dy, 0]
+        for k in range(1, n):
+            total = total + got_sq[dy, k]
+        inv_row = lax.rsqrt(total / full_width + norm_eps)
+        inv_two = jnp.sum(jnp.where(square, inv_row, 0.0), axis=1, keepdims=True)
+        x_up[dy].wait_all()
         total = got_up[0, at].astype(f32)
         for k in range(1, n):
             total = total + got_up[k, at].astype(f32)
-        pre = jnp.maximum(total * inv_two[c * R : (c + 1) * R], 0.0)
+        pre = jnp.maximum(total * inv_two, 0.0)
         mine_act[at, :] = (pre * pre).astype(bf16)
-        x_act[c].start_all()
+        x_act[dy].start_all()
         all_act[me, at] = mine_act[at, :]
 
     x_down = ex("tp", 10, lambda p: down_v.at[rows_of(p * B, B)], got_down)
-    for c in range(CHUNKS):
-        at = pl.ds(c * R, R)
-        x_act[c].wait_all()
+    for dy, (y, at) in enumerate(zip(chips, ats)):
+        x_act[dy].wait_all()
         act = jnp.concatenate([all_act[k, at] for k in range(n)], axis=1)
         down_v[at, :] = jnp.dot(act, wd_v[...], preferred_element_type=f32).astype(bf16)
-        for p in range(c * R // B, (c + 1) * R // B):
-
-            @pl.when(my_tp != p)
-            def _(p=p):
-                x_down.copy(p).start()
-
+        for peer in [y * 2, y * 2 + 1] if dy else [y * 2 + 1 - my_c]:
+            x_down.copy(peer).start()
     got_down[my_tp] = down_v[rows_of(my_tp * B, B), :]
     x_down.wait_all()
     total = got_down[0].astype(f32)
@@ -449,7 +460,10 @@
     mixed[...] = (res_v[...].astype(f32) + total).astype(bf16)
 
     x_kv2.wait_all()
-    for x in [x_s, x_q, x_kv, x_q2, x_kv2, x_acc, x_stat, x_n, x_res, x_sq, x_down] + x_up + x_act:
+    sent = all_res.at[pl.ds(0, n_tp - 1)]
+    remote(sent, sent, res_sent, res_sem.at[0], "tp", tp_peers[0]).wait_send()
+    once = [x_s, x_q, x_kv, x_far, x_near, x_kv2, x_acc, x_stat, x_n, x_down]
+    for x in once + x_sq + x_up + x_act:
         x.drain()
 
 
@@ -531,15 +545,16 @@
         V((B * heads, vd), f32),
         V((B, tok_width), bf16),
         V((n_tp, B, tok_width), bf16),
-        V((1, all_rows), f32),
-        V((n, 1, all_rows), f32),
+        V((n_tp // 2, 1, 128), f32),
+        V((n_tp // 2, n, 1, 128), f32),
         V((n, all_rows, cw), bf16),
         V((n, all_rows, cw), bf16),
         V((all_rows, cw), bf16),
         V((n, all_rows, cw), bf16),
         V((all_rows, tok_width), bf16),
         V((n_tp, B, tok_width), bf16),
-        DMA((11 + 2 * CHUNKS, 2)),
+        DMA((11 + 3 * (n_tp // 2), 2)),
+        DMA((n_tp // 2,)),
     ]
     mixed, kv_out = pl.pallas_call(
         functools.partial(

time: 61.1 us -> 55.1 us (0.902)
  Pallas kernels: 60.3 us -> 54.3 us
    pallas_call x1, Pallas kernels: 59.7 us -> 53.6 us  [shards(): pl.pallas_call(functools.partial(layer_kernel, n, n_tp, kv_heads, tok_wid...]
where the time goes in v3:
time: 55.1 us; the launch traced here: 54.9 us
  Pallas kernels  54.3 us (99%)
  between operations  0.64 us (1%)
    pallas_call x1, Pallas kernels, shards(): pl.pallas_call(functools.partial(layer_kernel, n, n_tp, kv_heads, tok_wid...  53.6 us

profile of v3, /device:TPU:1, one launch (start us, length us, event | category | flops | bytes accessed | tf_op | source)
XLA Modules:
  0.0 54.9 jit_solution(16207449570594108709)
XLA Ops:
  0.6 53.6 %shard_map.148 = (bf16[16,256]{1,0:T(8,128)(2,1)S(1)}, bf16[16,2,2,128]{3,2,1,0:T(2,128)(2,1)S(1)}) custom-call(bf16[16,256]{1,0:T(8,128)(2,1)} %tokens.1, bf16[16,2048,128]{2,1,0:T(8,128)(2,1)} %bitcast.6, bf16[16,2048,128]{2,1,0:T(8,128)(2,1)} %bitcast.7, f32[1,256]{1,0:T(1,128)} %bitcast.8, bf16[256,2048]{1,0:T(8,128)(2,1)} %w_query.1, ...), custom_call_target="tpu_custom_call" | custom-call | tf_op jit(solution)/shard_map/pallas_call | solution.py:559
  54.3 0.6 %shard_map.149 = (bf16[16,256]{1,0:T(8,128)(2,1)}, bf16[16,2,128]{2,1,0:T(2,128)(2,1)}, bf16[16,2,128]{2,1,0:T(2,128)(2,1)}) custom-call(bf16[16,256]{1,0:T(8,128)(2,1)S(1)} %get-tuple-element.5.mixed, bf16[16,2,2,128]{3,2,1,0:T(2,128)(2,1)S(1)} %get-tuple-element.6.kv_out), custom_call_target="tpu_custom_call" | custom-call | tf_op jit(solution)/shard_map/pallas_call | solution.py:593

commit v4 on v3

--- a/solution.py
+++ b/solution.py
@@ -15,6 +15,8 @@
 DMA = pltpu.SemaphoreType.DMA
 NT = (((1,), (1,)), ((), ()))
 UNROLL = 4
+AHEAD = 2
+BEHIND = 1
 
 
 def remote(src, dst, send, recv, axis, peer):
@@ -188,15 +190,9 @@
     for c in first:
         c.wait()
 
-    def fetch(b):
-        return (
-            pltpu.make_async_copy(keys.at[b], kbuf.at[b], ksem),
-            pltpu.make_async_copy(values.at[b], vbuf.at[b], vsem),
-        )
-
-    for b in kv_order:
-        for c in fetch(b):
-            c.start()
+    for src, dst, sem in ((keys, kbuf, ksem), (values, vbuf, vsem)):
+        for b in kv_order:
+            pltpu.make_async_copy(src.at[b], dst.at[b], sem).start()
     for c in later:
         c.start()
 
@@ -265,12 +261,14 @@
     x_acc = ex("kv", 5, lambda p: acc.at[p], gacc)
     x_stat = ex("kv", 6, lambda p: stat.at[p], gstat)
 
-    def one_row(b):
+    def scores_of(b):
         q = all_q[b].astype(f32)
         lo = jnp.where(low, q, 0.0)
         hi = jnp.where(low, 0.0, q)
         q_lines = jnp.concatenate([lo[:half], hi[:half], lo[half:], hi[half:]], axis=0).astype(bf16)
-        s = lax.dot_general(q_lines, kbuf[b], NT, preferred_element_type=f32)
+        return lax.dot_general(q_lines, kbuf[b], NT, preferred_element_type=f32)
+
+    def softmax_of(s):
         m = [
             jnp.where(even, s[:heads, c * 128 : (c + 1) * 128], s[heads:, c * 128 : (c + 1) * 128])
             for c in range(groups)
@@ -294,17 +292,22 @@
             ],
             axis=0,
         )
-        o = jnp.dot(e, vbuf[b], preferred_element_type=f32)
         tops = jnp.concatenate([top0, top1], axis=0)
         tots = jnp.concatenate([tot0, tot1], axis=0)
         row0 = jnp.sum(jnp.where(diag, tops, 0.0), axis=0, keepdims=True)
         row1 = jnp.sum(jnp.where(diag, tots, 0.0), axis=0, keepdims=True)
-        return o.astype(bf16), jnp.concatenate([row0, row1], axis=0)
+        return e, jnp.concatenate([row0, row1], axis=0)
 
     def attend(bs, send=True):
-        for b, (o, st) in zip(bs, [one_row(b) for b in bs]):
-            acc[b] = o
-            stat[b] = st
+        s, e = {}, {}
+        for i in range(-AHEAD, len(bs) + BEHIND):
+            if i + AHEAD < len(bs):
+                s[i + AHEAD] = scores_of(bs[i + AHEAD])
+            if 0 <= i < len(bs):
+                e[i], stat[bs[i]] = softmax_of(s.pop(i))
+            if i >= BEHIND:
+                b = bs[i - BEHIND]
+                acc[b] = jnp.dot(e.pop(i - BEHIND), vbuf[b], preferred_element_type=f32).astype(bf16)
         for b in bs if send else ():
             x_acc.copy(b).start()
             x_stat.copy(b).start()

time: 55.1 us -> 52.4 us (0.951)
  Pallas kernels: 54.3 us -> 51.6 us
    pallas_call x1, Pallas kernels: 53.6 us -> 51 us  [shards(): pl.pallas_call(functools.partial(layer_kernel, n, n_tp, kv_heads, tok_wid...]
where the time goes in v4:
time: 52.4 us; the launch traced here: 52.3 us
  Pallas kernels  51.6 us (98%)
  between operations  0.64 us (1%)
    pallas_call x1, Pallas kernels, shards(): pl.pallas_call(functools.partial(layer_kernel, n, n_tp, kv_heads, tok_wid...  51 us

profile of v4, /device:TPU:1, one launch (start us, length us, event | category | flops | bytes accessed | tf_op | source)
XLA Modules:
  0.0 52.3 jit_solution(17246838034294603001)
XLA Ops:
  0.6 51.0 %shard_map.148 = (bf16[16,256]{1,0:T(8,128)(2,1)S(1)}, bf16[16,2,2,128]{3,2,1,0:T(2,128)(2,1)S(1)}) custom-call(bf16[16,256]{1,0:T(8,128)(2,1)} %tokens.1, bf16[16,2048,128]{2,1,0:T(8,128)(2,1)} %bitcast.6, bf16[16,2048,128]{2,1,0:T(8,128)(2,1)} %bitcast.7, f32[1,256]{1,0:T(1,128)} %bitcast.8, bf16[256,2048]{1,0:T(8,128)(2,1)} %w_query.1, ...), custom_call_target="tpu_custom_call" | custom-call | tf_op jit(solution)/shard_map/pallas_call | solution.py:562
  51.6 0.6 %shard_map.149 = (bf16[16,256]{1,0:T(8,128)(2,1)}, bf16[16,2,128]{2,1,0:T(2,128)(2,1)}, bf16[16,2,128]{2,1,0:T(2,128)(2,1)}) custom-call(bf16[16,256]{1,0:T(8,128)(2,1)S(1)} %get-tuple-element.5.mixed, bf16[16,2,2,128]{3,2,1,0:T(2,128)(2,1)S(1)} %get-tuple-element.6.kv_out), custom_call_target="tpu_custom_call" | custom-call | tf_op jit(solution)/shard_map/pallas_call | solution.py:596

commit v5 on v4

--- a/solution.py
+++ b/solution.py
@@ -16,6 +16,7 @@
 NT = (((1,), (1,)), ((), ()))
 UNROLL = 4
 AHEAD = 2
+FLIPPED = 8
 BEHIND = 1
 
 
@@ -134,6 +135,7 @@
     got_down,
     sems,
     res_sem,
+    flipped,
 ):
     me = lax.axis_index("kv")
     my_tp = lax.axis_index("tp")
@@ -190,9 +192,30 @@
     for c in first:
         c.wait()
 
-    for src, dst, sem in ((keys, kbuf, ksem), (values, vbuf, vsem)):
-        for b in kv_order:
-            pltpu.make_async_copy(src.at[b], dst.at[b], sem).start()
+    for i, b in enumerate(kv_order):
+        pltpu.make_async_copy(keys.at[b], kbuf.at[b], ksem.at[i // FLIPPED]).start()
+    for b in kv_order:
+        pltpu.make_async_copy(values.at[b], vbuf.at[b], vsem).start()
+
+    def keys_wait(i):
+        first, size = i * FLIPPED, min(FLIPPED, B - i * FLIPPED)
+        at = pl.ds(first, size)
+        pltpu.make_async_copy(keys.at[at], kbuf.at[at], ksem.at[i]).wait()
+
+    eye = jnp.where(
+        lax.broadcasted_iota(jnp.int32, (128, 128), 0)
+        == lax.broadcasted_iota(jnp.int32, (128, 128), 1),
+        1.0,
+        0.0,
+    ).astype(bf16)
+
+    def flip():
+        keys_wait(0)
+        for i in range(FLIPPED):
+            flipped[i] = lax.dot_general(
+                eye, kbuf[kv_order[i]], NT, preferred_element_type=f32
+            ).astype(bf16)
+
     for c in later:
         c.start()
 
@@ -224,6 +247,7 @@
     got_q[me] = part_q[rows_of(me * heads, heads), :]
     got_s[me] = part_s[me]
     got_kv[me] = part_kv[rows_of(me * 8, 8), :]
+    flip()
     x_s.wait_all()
     total = got_s[0]
     for k in range(1, n):
@@ -266,6 +290,9 @@
         lo = jnp.where(low, q, 0.0)
         hi = jnp.where(low, 0.0, q)
         q_lines = jnp.concatenate([lo[:half], hi[:half], lo[half:], hi[half:]], axis=0).astype(bf16)
+        for i in range(FLIPPED):
+            if b is kv_order[i]:
+                return jnp.dot(q_lines, flipped[i], preferred_element_type=f32)
         return lax.dot_general(q_lines, kbuf[b], NT, preferred_element_type=f32)
 
     def softmax_of(s):
@@ -312,7 +339,8 @@
             x_acc.copy(b).start()
             x_stat.copy(b).start()
 
-    pltpu.make_async_copy(keys, kbuf, ksem).wait()
+    for i in range(1, -(-B // FLIPPED)):
+        keys_wait(i)
     pltpu.make_async_copy(values, vbuf, vsem).wait()
     attend([me], send=False)
     x_near.wait_all()
@@ -528,7 +556,7 @@
         V(w_up.shape, bf16),
         V(w_down.shape, bf16),
         DMA((11,)),
-        DMA,
+        DMA((-(-B // FLIPPED),)),
         DMA,
         V((B * heads, 128), f32),
         V((B, 1, 128), f32),
@@ -558,6 +586,7 @@
         V((n_tp, B, tok_width), bf16),
         DMA((11 + 3 * (n_tp // 2), 2)),
         DMA((n_tp // 2,)),
+        V((FLIPPED, 128, span), bf16),
     ]
     mixed, kv_out = pl.pallas_call(
         functools.partial(

time: 52.4 us -> 51.5 us (0.983)
  Pallas kernels: 51.6 us -> 50.7 us
    pallas_call x1, Pallas kernels: 51 us -> 50.1 us  [shards(): pl.pallas_call(functools.partial(layer_kernel, n, n_tp, kv_heads, tok_wid...]
where the time goes in v5:
time: 51.5 us; the launch traced here: 51.4 us
  Pallas kernels  50.7 us (98%)
  between operations  0.64 us (1%)
    pallas_call x1, Pallas kernels, shards(): pl.pallas_call(functools.partial(layer_kernel, n, n_tp, kv_heads, tok_wid...  50.1 us

profile of v5, /device:TPU:1, one launch (start us, length us, event | category | flops | bytes accessed | tf_op | source)
XLA Modules:
  0.0 51.4 jit_solution(2822286188363557027)
XLA Ops:
  0.6 50.1 %shard_map.148 = (bf16[16,256]{1,0:T(8,128)(2,1)S(1)}, bf16[16,2,2,128]{3,2,1,0:T(2,128)(2,1)S(1)}) custom-call(bf16[16,256]{1,0:T(8,128)(2,1)} %tokens.1, bf16[16,2048,128]{2,1,0:T(8,128)(2,1)} %bitcast.6, bf16[16,2048,128]{2,1,0:T(8,128)(2,1)} %bitcast.7, f32[1,256]{1,0:T(1,128)} %bitcast.8, bf16[256,2048]{1,0:T(8,128)(2,1)} %w_query.1, ...), custom_call_target="tpu_custom_call" | custom-call | tf_op jit(solution)/shard_map/pallas_call | solution.py:591
  50.7 0.6 %shard_map.149 = (bf16[16,256]{1,0:T(8,128)(2,1)}, bf16[16,2,128]{2,1,0:T(2,128)(2,1)}, bf16[16,2,128]{2,1,0:T(2,128)(2,1)}) custom-call(bf16[16,256]{1,0:T(8,128)(2,1)S(1)} %get-tuple-element.5.mixed, bf16[16,2,2,128]{3,2,1,0:T(2,128)(2,1)S(1)} %get-tuple-element.6.kv_out), custom_call_target="tpu_custom_call" | custom-call | tf_op jit(solution)/shard_map/pallas_call | solution.py:625

commit v6 on v5

--- a/solution.py
+++ b/solution.py
@@ -16,7 +16,7 @@
 NT = (((1,), (1,)), ((), ()))
 UNROLL = 4
 AHEAD = 2
-FLIPPED = 8
+FLIPPED = 11
 BEHIND = 1
 
 
@@ -35,7 +35,7 @@
     def __init__(self, axis, peers, me, src_of, dst_of, all_dst, sems):
         self.axis, self.peers, self.me = axis, peers, me
         self.src_of, self.dst_of, self.all_dst = src_of, dst_of, all_dst
-        self.send, self.recv = sems.at[0], sems.at[1]
+        self.send, self.recv = sems
 
     def copy(self, peer):
         return remote(
@@ -135,6 +135,7 @@
     got_down,
     sems,
     res_sem,
+    sent,
     flipped,
 ):
     me = lax.axis_index("kv")
@@ -167,7 +168,7 @@
         every, at = (kv_peers, me) if axis == "kv" else (tp_peers, my_tp)
         peers = every if peers is None else peers
         return Exchange(
-            axis, peers, at, src_of, lambda p: dst.at[p], dst.at[pl.ds(0, len(peers))], sems.at[i]
+            axis, peers, at, src_of, lambda p: dst.at[p], dst.at[pl.ds(0, len(peers))], (sent, sems.at[i])
         )
 
     first = [(tokens, tok_v), (attn_gain, ag_v), (w_query, wq_v), (w_key, wk_v), (w_value, wv_v)]
@@ -189,13 +190,13 @@
             pl.semaphore_signal(
                 barrier, inc=1, device_id={axis: peer}, device_id_type=pl.DeviceIdType.MESH
             )
-    for c in first:
-        c.wait()
-
     for i, b in enumerate(kv_order):
         pltpu.make_async_copy(keys.at[b], kbuf.at[b], ksem.at[i // FLIPPED]).start()
     for b in kv_order:
         pltpu.make_async_copy(values.at[b], vbuf.at[b], vsem).start()
+
+    for c in first:
+        c.wait()
 
     def keys_wait(i):
         first, size = i * FLIPPED, min(FLIPPED, B - i * FLIPPED)
@@ -400,7 +401,7 @@
     attn_out = jnp.dot(normed, wo_v[...], preferred_element_type=f32)
     res_v[...] = (tok_v[...].astype(f32) + attn_out).astype(bf16)
     my_y, my_c = my_tp // 2, lax.rem(my_tp, 2)
-    res_sent = sems.at[9, 0]
+    res_sent = sent
 
     def res_copy(dy, dc):
         peer = lax.rem(my_y + dy, ny) * 2 + lax.rem(my_c + dc, 2)
@@ -426,7 +427,7 @@
                 lambda p, dy=dy: sq_v.at[dy],
                 lambda p, dy=dy: got_sq.at[dy, p],
                 got_sq.at[dy, pl.ds(0, n - 1)],
-                sems.at[11 + 3 * dy],
+                (sent, sems.at[11 + 3 * dy]),
             )
         )
         for xs, src_of, dst, i in (
@@ -441,7 +442,7 @@
                     src_of,
                     lambda p, dst=dst, at=at: dst.at[p, at],
                     dst.at[pl.ds(0, n - 1), at],
-                    sems.at[i],
+                    (sent, sems.at[i]),
                 )
             )
 
@@ -584,8 +585,9 @@
         V((n, all_rows, cw), bf16),
         V((all_rows, tok_width), bf16),
         V((n_tp, B, tok_width), bf16),
-        DMA((11 + 3 * (n_tp // 2), 2)),
+        DMA((11 + 3 * (n_tp // 2),)),
         DMA((n_tp // 2,)),
+        DMA,
         V((FLIPPED, 128, span), bf16),
     ]
     mixed, kv_out = pl.pallas_call(

time: 51.5 us -> 50.9 us (0.988)
    pallas_call x1, Pallas kernels: 50.1 us -> 49.5 us  [shards(): pl.pallas_call(functools.partial(layer_kernel, n, n_tp, kv_heads, tok_wid...]
where the time goes in v6:
time: 50.9 us; the launch traced here: 50.8 us
  Pallas kernels  50.2 us (99%)
  between operations  0.64 us (1%)
    pallas_call x1, Pallas kernels, shards(): pl.pallas_call(functools.partial(layer_kernel, n, n_tp, kv_heads, tok_wid...  49.5 us

profile of v6, /device:TPU:1, one launch (start us, length us, event | category | flops | bytes accessed | tf_op | source)
XLA Modules:
  0.0 50.8 jit_solution(12674966579692595575)
XLA Ops:
  0.6 49.5 %shard_map.148 = (bf16[16,256]{1,0:T(8,128)(2,1)S(1)}, bf16[16,2,2,128]{3,2,1,0:T(2,128)(2,1)S(1)}) custom-call(bf16[16,256]{1,0:T(8,128)(2,1)} %tokens.1, bf16[16,2048,128]{2,1,0:T(8,128)(2,1)} %bitcast.6, bf16[16,2048,128]{2,1,0:T(8,128)(2,1)} %bitcast.7, f32[1,256]{1,0:T(1,128)} %bitcast.8, bf16[256,2048]{1,0:T(8,128)(2,1)} %w_query.1, ...), custom_call_target="tpu_custom_call" | custom-call | tf_op jit(solution)/shard_map/pallas_call | solution.py:593
  50.2 0.6 %shard_map.149 = (bf16[16,256]{1,0:T(8,128)(2,1)}, bf16[16,2,128]{2,1,0:T(2,128)(2,1)}, bf16[16,2,128]{2,1,0:T(2,128)(2,1)}) custom-call(bf16[16,256]{1,0:T(8,128)(2,1)S(1)} %get-tuple-element.5.mixed, bf16[16,2,2,128]{3,2,1,0:T(2,128)(2,1)S(1)} %get-tuple-element.6.kv_out), custom_call_target="tpu_custom_call" | custom-call | tf_op jit(solution)/shard_map/pallas_call | solution.py:627

commit v7 on v6

--- a/solution.py
+++ b/solution.py
@@ -15,7 +15,7 @@
 DMA = pltpu.SemaphoreType.DMA
 NT = (((1,), (1,)), ((), ()))
 UNROLL = 4
-AHEAD = 2
+AHEAD = 3
 FLIPPED = 11
 BEHIND = 1
 

time: 50.9 us -> 50.9 us (level)
  no operation moved by 1% of the time
where the time goes in v7:
time: 50.9 us; the launch traced here: 50.8 us
  Pallas kernels  50.2 us (99%)
  between operations  0.64 us (1%)
    pallas_call x1, Pallas kernels, shards(): pl.pallas_call(functools.partial(layer_kernel, n, n_tp, kv_heads, tok_wid...  49.5 us

profile of v7, /device:TPU:1, one launch (start us, length us, event | category | flops | bytes accessed | tf_op | source)
XLA Modules:
  0.0 50.8 jit_solution(12674966579692595575)
XLA Ops:
  0.6 49.5 %shard_map.148 = (bf16[16,256]{1,0:T(8,128)(2,1)S(1)}, bf16[16,2,2,128]{3,2,1,0:T(2,128)(2,1)S(1)}) custom-call(bf16[16,256]{1,0:T(8,128)(2,1)} %tokens.1, bf16[16,2048,128]{2,1,0:T(8,128)(2,1)} %bitcast.6, bf16[16,2048,128]{2,1,0:T(8,128)(2,1)} %bitcast.7, f32[1,256]{1,0:T(1,128)} %bitcast.8, bf16[256,2048]{1,0:T(8,128)(2,1)} %w_query.1, ...), custom_call_target="tpu_custom_call" | custom-call | tf_op jit(solution)/shard_map/pallas_call | solution.py:593
  50.2 0.6 %shard_map.149 = (bf16[16,256]{1,0:T(8,128)(2,1)}, bf16[16,2,128]{2,1,0:T(2,128)(2,1)}, bf16[16,2,128]{2,1,0:T(2,128)(2,1)}) custom-call(bf16[16,256]{1,0:T(8,128)(2,1)S(1)} %get-tuple-element.5.mixed, bf16[16,2,2,128]{3,2,1,0:T(2,128)(2,1)S(1)} %get-tuple-element.6.kv_out), custom_call_target="tpu_custom_call" | custom-call | tf_op jit(solution)/shard_map/pallas_call | solution.py:627

commit v8 on v7

--- a/solution.py
+++ b/solution.py
@@ -14,10 +14,10 @@
 HBM = pl.BlockSpec(memory_space=pltpu.HBM)
 DMA = pltpu.SemaphoreType.DMA
 NT = (((1,), (1,)), ((), ()))
-UNROLL = 4
+UNROLL = 6
 AHEAD = 3
 FLIPPED = 11
-BEHIND = 1
+BEHIND = 2
 
 
 def remote(src, dst, send, recv, axis, peer):

time: 50.9 us -> 51 us (level)
  no operation moved by 1% of the time
where the time goes in v8:
time: 51 us; the launch traced here: 50.9 us
  Pallas kernels  50.2 us (98%)
  between operations  0.64 us (1%)
    pallas_call x1, Pallas kernels, shards(): pl.pallas_call(functools.partial(layer_kernel, n, n_tp, kv_heads, tok_wid...  49.6 us

profile of v8, /device:TPU:1, one launch (start us, length us, event | category | flops | bytes accessed | tf_op | source)
XLA Modules:
  0.0 50.9 jit_solution(17601325029471482922)
XLA Ops:
  0.6 49.6 %shard_map.148 = (bf16[16,256]{1,0:T(8,128)(2,1)S(1)}, bf16[16,2,2,128]{3,2,1,0:T(2,128)(2,1)S(1)}) custom-call(bf16[16,256]{1,0:T(8,128)(2,1)} %tokens.1, bf16[16,2048,128]{2,1,0:T(8,128)(2,1)} %bitcast.6, bf16[16,2048,128]{2,1,0:T(8,128)(2,1)} %bitcast.7, f32[1,256]{1,0:T(1,128)} %bitcast.8, bf16[256,2048]{1,0:T(8,128)(2,1)} %w_query.1, ...), custom_call_target="tpu_custom_call" | custom-call | tf_op jit(solution)/shard_map/pallas_call | solution.py:593
  50.3 0.6 %shard_map.149 = (bf16[16,256]{1,0:T(8,128)(2,1)}, bf16[16,2,128]{2,1,0:T(2,128)(2,1)}, bf16[16,2,128]{2,1,0:T(2,128)(2,1)}) custom-call(bf16[16,256]{1,0:T(8,128)(2,1)S(1)} %get-tuple-element.5.mixed, bf16[16,2,2,128]{3,2,1,0:T(2,128)(2,1)S(1)} %get-tuple-element.6.kv_out), custom_call_target="tpu_custom_call" | custom-call | tf_op jit(solution)/shard_map/pallas_call | solution.py:627
